TPU v7x, 768 devices: a whole 4x8x12 slice. The times are simulated.
768 devices in a mesh: sp: 384 (over z, y, x), tp: 2 (over core).
Axes of the slice: x: 4, y: 8, z: 12, core: 2. Of those that a mesh axis runs over, the one named last changes fastest.
Arguments:
- queries: bfloat16 [98304, 1024], P('sp', 'tp'), may hold values from -12 to 12
- keys: bfloat16 [98304, 1024], P('sp', 'tp'), may hold values from -6 to 6
- values: bfloat16 [98304, 1024], P('sp', 'tp'), may hold values from -6 to 6
- w_out: bfloat16 [1024, 2048], P(None, 'tp'), may hold values from -0.375 to 0.375
Outputs:
- mixed: bfloat16 [98304, 2048], P('sp', 'tp')
All inputs are finite; a program needn't handle non-finite values.
Results may differ from a plain program's by a relative error of at most 0.0056.
Values may be sent and summed in bfloat16 or wider, within the bound.
A program may use at most 64 MiB of HBM per device.

v0:
```python
import jax
import jax.numpy as jnp
from jax import lax
from jax.sharding import PartitionSpec as P

HEAD_DIM = 128
SIDE_KEY_COUNT = 64
MIDDLE_DILATION = 4
FAR_DILATION = 16


def from_behind(value, axis, steps):
    count = lax.axis_size(axis)
    first, last = (max(0, -steps), min(count, count - steps))
    return lax.ppermute(value, axis, [(source, source + steps) for source in range(first, last)])


def sent_to_all(x, axis):
    size = lax.axis_size(axis)
    return lax.all_to_all(jnp.broadcast_to(x[None], (size, *x.shape)), axis, 0, 0, tiled=True)


def in_order(tiles, dim):
    tiles = jnp.moveaxis(tiles, 0, dim)
    lengths = tiles.shape
    return tiles.reshape(*lengths[:dim], lengths[dim] * lengths[dim + 1], *lengths[dim + 2 :])


def gather_directly(x, axis, dim):
    tiles = sent_to_all(x, axis)
    return in_order(tiles, dim)


def band_scores(queries, window_keys, start_position, sequence_length, dilation_step):
    nearby_rows, columns = queries.shape
    heads = columns // HEAD_DIM
    residue_rows = nearby_rows // dilation_step
    blocks = residue_rows // residue_rows
    span = residue_rows + 2 * SIDE_KEY_COUNT
    laid = jnp.transpose(
        window_keys.reshape(2, residue_rows + 2 * SIDE_KEY_COUNT, dilation_step, heads, HEAD_DIM),
        (0, 2, 3, 1, 4),
    )
    grouped = jnp.transpose(
        queries.reshape(blocks, residue_rows, dilation_step, heads, HEAD_DIM), (0, 2, 3, 1, 4)
    )
    query_idx = jnp.arange(residue_rows, dtype=jnp.int32)[:, None]
    key_idx = jnp.arange(span, dtype=jnp.int32)[None, :]
    in_band = (key_idx >= query_idx) & (key_idx <= query_idx + 2 * SIDE_KEY_COUNT)
    residues = jnp.arange(dilation_step, dtype=jnp.int32)[:, None, None, None]
    scale = HEAD_DIM ** (-0.5)

    def one_block(inputs):
        number, query_block = inputs
        first_row = number * residue_rows
        scores = (
            jnp.einsum("rhqe,rhke->rhqk", query_block, laid[0], preferred_element_type=jnp.float32)
            * scale
        )
        key_pos = (
            start_position
            + (first_row + key_idx[None, None] - SIDE_KEY_COUNT) * dilation_step
            + residues
        )
        allowed = in_band[None, None] & (key_pos >= 0) & (key_pos < sequence_length)
        scores = jnp.where(allowed, scores, -jnp.inf)
        maximum = jnp.max(scores, axis=-1, keepdims=True)
        raised = jnp.exp(scores - maximum)
        denominator = jnp.sum(raised, axis=-1, keepdims=True)
        weights = (raised / denominator).astype(jnp.bfloat16)
        attended = jnp.einsum(
            "rhqk,rhke->rhqe", weights, laid[1], preferred_element_type=jnp.float32
        )
        log_den = (maximum + jnp.log(denominator))[..., 0]
        return (attended, log_den)

    outputs, log_dens = lax.map(one_block, (jnp.arange(blocks, dtype=jnp.int32), grouped))
    attended = jnp.transpose(outputs, (0, 3, 1, 2, 4)).reshape(nearby_rows, heads, HEAD_DIM)
    log_den = jnp.transpose(log_dens, (0, 3, 1, 2)).reshape(nearby_rows, heads)
    return (attended, log_den)


def far_blocks(stacked_groups, hop_count):
    sides = []
    for direction in (1, -1):
        current = stacked_groups
        received = []
        for counter in range(hop_count):
            current = from_behind(current, "sp", direction)
            received.append(current)
        sides.append(received)
    return sides[0][::-1] + [stacked_groups] + sides[1]


def per_device(queries, keys, values, w_out):
    nearby_rows, columns = queries.shape
    sequence_length = nearby_rows * lax.axis_size("sp")
    start_position = lax.axis_index("sp") * nearby_rows
    stacked_groups = jnp.stack([keys, values])
    hop_count = -(-(SIDE_KEY_COUNT * FAR_DILATION) // nearby_rows)
    extended = jnp.concatenate(far_blocks(stacked_groups, hop_count), axis=1)

    def window_keys(dilation_step):
        padding = SIDE_KEY_COUNT * dilation_step
        return lax.slice_in_dim(
            extended,
            hop_count * nearby_rows - padding,
            (hop_count + 1) * nearby_rows + padding,
            axis=1,
        )

    nearby = window_keys(1)
    middle_group = window_keys(MIDDLE_DILATION)
    distant_group = window_keys(FAR_DILATION)
    group_results = [
        band_scores(queries, nearby, start_position, sequence_length, 1),
        band_scores(queries, middle_group, start_position, sequence_length, MIDDLE_DILATION),
        band_scores(queries, distant_group, start_position, sequence_length, FAR_DILATION),
    ]
    stacked_out = jnp.stack([item[0] for item in group_results])
    stacked_den = jnp.stack([item[1] for item in group_results])
    shares = jax.nn.softmax(stacked_den, axis=0)
    attended = (
        jnp.sum(shares[..., None] * stacked_out, axis=0)
        .astype(jnp.bfloat16)
        .reshape(nearby_rows, columns)
    )
    mixed = jnp.dot(gather_directly(attended, "tp", 1), w_out, preferred_element_type=jnp.float32)
    return mixed.astype(jnp.bfloat16)


def solution(mesh):
    in_specs = (P("sp", "tp"), P("sp", "tp"), P("sp", "tp"), P(None, "tp"))
    out_specs = P("sp", "tp")
    return jax.shard_map(
        per_device, mesh=mesh, in_specs=in_specs, out_specs=out_specs, check_vma=False
    )
```

profile of v0, /device:TPU:513, one launch (start us, length us, event | category | flops | bytes accessed | tf_op | source)
XLA Modules:
  0.0 142.8 jit_solution(15584434611720476525)
XLA Ops:
  3.2 3.1 %collective-permute-start = (bf16[2,256,512]{1,2,0:T(8,128)(2,1)}, bf16[2,256,512]{1,2,0:T(8,128)(2,1)S(1)}, u32[]{:S(2)}, u32[]{:S(2)}) collective-permute-start(bf16[2,256,512]{1,2,0:T(8,128)(2,1)} %pad_maximum_fusion.1), channel_id=1, source_target_pairs={{0,2},{2,4},{4,6},{6,8},{8,10},{10,12},{12,14},{14,16},{16,18},{18... | collective-permute-start | bytes 1572872 | tf_op jit(solution)/shard_map/ppermute | solution.py:15
  6.3 7.6 %collective-permute-start.1 = (bf16[2,256,512]{1,2,0:T(8,128)(2,1)}, bf16[2,256,512]{1,2,0:T(8,128)(2,1)}, u32[]{:S(2)}, u32[]{:S(2)}) collective-permute-start(bf16[2,256,512]{1,2,0:T(8,128)(2,1)} %pad_maximum_fusion.1), channel_id=1, source_target_pairs={{2,0},{4,2},{6,4},{8,6},{10,8},{12,10},{14,12},{16,14},{18,16},{20... | collective-permute-start | bytes 1572872 | tf_op jit(solution)/shard_map/ppermute | solution.py:15
  18.9 4.6 %collective-permute-done = bf16[2,256,512]{1,2,0:T(8,128)(2,1)S(1)} collective-permute-done((bf16[2,256,512]{1,2,0:T(8,128)(2,1)}, bf16[2,256,512]{1,2,0:T(8,128)(2,1)S(1)}, u32[]{:S(2)}, u32[]{:S(2)}) %collective-permute-start) | collective-permute-done | bytes 524320 | tf_op jit(solution)/shard_map/ppermute | solution.py:15
  24.5 2.3 %pad_maximum_fusion = bf16[2,768,512]{1,2,0:T(8,128)(2,1)} fusion(bf16[2,256,512]{1,2,0:T(8,128)(2,1)} %collective-permute-done.1, bf16[1,256,512]{1,2,0:T(8,128)(2,1)S(1)} %bitcast.136, bf16[1,256,512]{1,2,0:T(8,128)(2,1)S(1)} %bitcast.133, bf16[2,256,512]{1,2,0:T(8,128)(2,1)S(1)} %collective-permute-done), kind=kLoop, calls=%fused_computation.5 | loop fusion | flops 6291456 | bytes 3145728 | tf_op jit(solution)/shard_map/concatenate | solution.py:101
  26.8 2.6 %copy.53 = bf16[2,768,512]{2,1,0:T(8,128)(2,1)} copy(bf16[2,768,512]{1,2,0:T(8,128)(2,1)} %pad_maximum_fusion) | data formatting | bytes 3145728 | tf_op jit(solution)/shard_map/concatenate | solution.py:101
  29.4 3.5 %reshape.469 = bf16[2,192,4,4,128]{4,3,2,1,0:T(4,128)(2,1)} reshape(bf16[2,768,512]{2,1,0:T(8,128)(2,1)} %copy.53) | data formatting | bytes 3145728 | tf_op jit(solution)/shard_map/reshape | solution.py:41
  34.8 1.9 %collective-permute-start.2 = (bf16[2,256,512]{1,2,0:T(8,128)(2,1)S(1)}, bf16[2,256,512]{1,2,0:T(8,128)(2,1)}, u32[]{:S(2)}, u32[]{:S(2)}) collective-permute-start(bf16[2,256,512]{1,2,0:T(8,128)(2,1)S(1)} %collective-permute-done), channel_id=1, source_target_pairs={{0,2},{2,4},{4,6},{6,8},{8,10},{10,12},{12,14},{14,16},{16,18},{18... | collective-permute-start | bytes 1572872 | tf_op jit(solution)/shard_map/ppermute | solution.py:15
  37.5 9.5 %collective-permute-start.5 = (bf16[2,256,512]{1,2,0:T(8,128)(2,1)}, bf16[2,256,512]{1,2,0:T(8,128)(2,1)}, u32[]{:S(2)}, u32[]{:S(2)}) collective-permute-start(bf16[2,256,512]{1,2,0:T(8,128)(2,1)} %collective-permute-done.1), channel_id=1, source_target_pairs={{2,0},{4,2},{6,4},{8,6},{10,8},{12,10},{14,12},{16,14},{18,16},{20... | collective-permute-start | bytes 1572872 | tf_op jit(solution)/shard_map/ppermute | solution.py:15
  48.7 6.2 %collective-permute-done.2 = bf16[2,256,512]{1,2,0:T(8,128)(2,1)} collective-permute-done((bf16[2,256,512]{1,2,0:T(8,128)(2,1)S(1)}, bf16[2,256,512]{1,2,0:T(8,128)(2,1)}, u32[]{:S(2)}, u32[]{:S(2)}) %collective-permute-start.2) | collective-permute-done | bytes 524320 | tf_op jit(solution)/shard_map/ppermute | solution.py:15
  54.9 1.9 %collective-permute-start.3 = (bf16[2,256,512]{1,2,0:T(8,128)(2,1)}, bf16[2,256,512]{1,2,0:T(8,128)(2,1)}, u32[]{:S(2)}, u32[]{:S(2)}) collective-permute-start(bf16[2,256,512]{1,2,0:T(8,128)(2,1)} %collective-permute-done.2), channel_id=1, source_target_pairs={{0,2},{2,4},{4,6},{6,8},{8,10},{10,12},{12,14},{14,16},{16,18},{18... | collective-permute-start | bytes 1572872 | tf_op jit(solution)/shard_map/ppermute | solution.py:15
  61.9 8.8 %collective-permute-start.6 = (bf16[2,256,512]{1,2,0:T(8,128)(2,1)}, bf16[2,256,512]{1,2,0:T(8,128)(2,1)S(1)}, u32[]{:S(2)}, u32[]{:S(2)}) collective-permute-start(bf16[2,256,512]{1,2,0:T(8,128)(2,1)} %collective-permute-done.5), channel_id=1, source_target_pairs={{2,0},{4,2},{6,4},{8,6},{10,8},{12,10},{14,12},{16,14},{18,16},{20... | collective-permute-start | bytes 1572872 | tf_op jit(solution)/shard_map/ppermute | solution.py:15
  70.7 2.9 %collective-permute-done.3 = bf16[2,256,512]{1,2,0:T(8,128)(2,1)} collective-permute-done((bf16[2,256,512]{1,2,0:T(8,128)(2,1)}, bf16[2,256,512]{1,2,0:T(8,128)(2,1)}, u32[]{:S(2)}, u32[]{:S(2)}) %collective-permute-start.3) | collective-permute-done | bytes 524320 | tf_op jit(solution)/shard_map/ppermute | solution.py:15
  73.7 1.9 %collective-permute-start.4 = (bf16[2,256,512]{1,2,0:T(8,128)(2,1)}, bf16[2,256,512]{1,2,0:T(8,128)(2,1)S(1)}, u32[]{:S(2)}, u32[]{:S(2)}) collective-permute-start(bf16[2,256,512]{1,2,0:T(8,128)(2,1)} %collective-permute-done.3), channel_id=1, source_target_pairs={{0,2},{2,4},{4,6},{6,8},{8,10},{10,12},{12,14},{14,16},{16,18},{18... | collective-permute-start | bytes 1572872 | tf_op jit(solution)/shard_map/ppermute | solution.py:15
  76.9 2.7 %collective-permute-done.6 = bf16[2,256,512]{1,2,0:T(8,128)(2,1)S(1)} collective-permute-done((bf16[2,256,512]{1,2,0:T(8,128)(2,1)}, bf16[2,256,512]{1,2,0:T(8,128)(2,1)S(1)}, u32[]{:S(2)}, u32[]{:S(2)}) %collective-permute-start.6) | collective-permute-done | bytes 524320 | tf_op jit(solution)/shard_map/ppermute | solution.py:15
  79.6 9.6 %collective-permute-start.7 = (bf16[2,256,512]{1,2,0:T(8,128)(2,1)S(1)}, bf16[2,256,512]{1,2,0:T(8,128)(2,1)S(1)}, u32[]{:S(2)}, u32[]{:S(2)}) collective-permute-start(bf16[2,256,512]{1,2,0:T(8,128)(2,1)S(1)} %collective-permute-done.6), channel_id=1, source_target_pairs={{2,0},{4,2},{6,4},{8,6},{10,8},{12,10},{14,12},{16,14},{18,16},{20... | collective-permute-start | bytes 1572872 | tf_op jit(solution)/shard_map/ppermute | solution.py:15
  89.2 2.2 %collective-permute-done.4 = bf16[2,256,512]{1,2,0:T(8,128)(2,1)S(1)} collective-permute-done((bf16[2,256,512]{1,2,0:T(8,128)(2,1)}, bf16[2,256,512]{1,2,0:T(8,128)(2,1)S(1)}, u32[]{:S(2)}, u32[]{:S(2)}) %collective-permute-start.4) | collective-permute-done | bytes 524320 | tf_op jit(solution)/shard_map/ppermute | solution.py:15
  92.3 2.0 %constant_dynamic-update-slice_fusion.7 = bf16[2,2304,512]{1,2,0:T(8,128)(2,1)} fusion(bf16[2,2304,512]{1,2,0:T(8,128)(2,1)} %constant_dynamic-update-slice_fusion.8, bf16[2,256,512]{1,2,0:T(8,128)(2,1)} %collective-permute-done.3), kind=kLoop, calls=%fused_computation.62 | loop fusion | bytes 1048576
  94.2 1.9 %constant_dynamic-update-slice_fusion.6 = bf16[2,2304,512]{1,2,0:T(8,128)(2,1)} fusion(bf16[2,2304,512]{1,2,0:T(8,128)(2,1)} %constant_dynamic-update-slice_fusion.7, bf16[2,256,512]{1,2,0:T(8,128)(2,1)} %collective-permute-done.2), kind=kLoop, calls=%fused_computation.61 | loop fusion | bytes 1048576
  97.9 1.9 %constant_dynamic-update-slice_fusion.3 = bf16[2,2304,512]{1,2,0:T(8,128)(2,1)} fusion(bf16[2,2304,512]{1,2,0:T(8,128)(2,1)} %constant_dynamic-update-slice_fusion.4, bf16[2,256,512]{1,2,0:T(8,128)(2,1)} %collective-permute-done.1), kind=kLoop, calls=%fused_computation.58 | loop fusion | bytes 1048576
  103.4 6.7 %copy.57 = bf16[2,2304,512]{2,1,0:T(8,128)(2,1)} copy(bf16[2,2304,512]{1,2,0:T(8,128)(2,1)} %constant_dynamic-update-slice_fusion) | data formatting | bytes 9437184 | tf_op jit(solution)/shard_map/concatenate | solution.py:101
  110.1 7.7 %reshape.471 = bf16[2,144,16,4,128]{4,3,2,1,0:T(4,128)(2,1)} reshape(bf16[2,2304,512]{2,1,0:T(8,128)(2,1)} %copy.57) | data formatting | bytes 9437184 | tf_op jit(solution)/shard_map/reshape | solution.py:41
  117.8 7.8 %copy.88 = bf16[2,144,16,4,128]{4,1,3,2,0:T(8,128)(2,1)S(1)} copy(bf16[2,144,16,4,128]{4,3,2,1,0:T(4,128)(2,1)} %reshape.471) | data formatting | bytes 9437184 | tf_op jit(solution)/shard_map/reshape | solution.py:41
  129.5 2.8 %fusion.9 = f32[1,16,16,4,128]{4,1,3,2,0:T(8,128)S(1)} fusion(bf16[2,16,4,144,128]{4,3,2,1,0:T(8,128)(2,1)} %bitcast.131, f32[16,4,16,144]{3,2,1,0:T(8,128)} %copy-done.6, f32[16,4,16]{2,1,0:T(4,128)S(1)} %fusion.11, f32[16,4,16]{2,1,0:T(4,128)S(1)} %get-tuple-element.58), kind=kOutput, calls=%fused_computation.22 | convolution fusion | flops 38191104 | bytes 3940352 | tf_op jit(solution)/shard_map/while/body/eval_jaxpr/rhqk,rhke->rhqe/dot_general | solution.py:71
  133.4 7.9 %all_to_all.5 = bf16[2,256,512]{1,2,0:T(8,128)(2,1)S(1)} all-to-all(bf16[2,256,512]{1,2,0:T(8,128)(2,1)S(1)} %broadcast_in_dim.121), channel_id=1, replica_groups=mesh['sp'=384,'tp'=2] {'tp'}, dimensions={0} | all-to-all | bytes 1048576 | tf_op jit(solution)/shard_map/all_to_all | solution.py:20
  (82 shorter events, 32.3 us)
Async XLA Ops:
  0.0 141.3 %copy-start = (bf16[1024,1024]{1,0:T(8,128)(2,1)S(1)}, bf16[1024,1024]{1,0:T(8,128)(2,1)}, u32[]{:S(2)}) copy-start(bf16[1024,1024]{1,0:T(8,128)(2,1)} %param.7) | copy-start | bytes 6291460
  0.0 15.7 %copy-start.3 = (bf16[256,512]{1,0:T(8,128)(2,1)S(1)}, bf16[256,512]{1,0:T(8,128)(2,1)}, u32[]{:S(2)}) copy-start(bf16[256,512]{1,0:T(8,128)(2,1)} %param.4) | copy-start | bytes 786436
  3.2 20.3 %collective-permute-start = (bf16[2,256,512]{1,2,0:T(8,128)(2,1)}, bf16[2,256,512]{1,2,0:T(8,128)(2,1)S(1)}, u32[]{:S(2)}, u32[]{:S(2)}) collective-permute-start(bf16[2,256,512]{1,2,0:T(8,128)(2,1)} %pad_maximum_fusion.1), channel_id=1, source_target_pairs={{0,2},{2,4},{4,6},{6,8},{8,10},{10,12},{12,14},{14,16},{16,18},{18... | collective-permute-start | bytes 1572872 | tf_op jit(solution)/shard_map/ppermute | solution.py:15
  6.3 18.2 %collective-permute-start.1 = (bf16[2,256,512]{1,2,0:T(8,128)(2,1)}, bf16[2,256,512]{1,2,0:T(8,128)(2,1)}, u32[]{:S(2)}, u32[]{:S(2)}) collective-permute-start(bf16[2,256,512]{1,2,0:T(8,128)(2,1)} %pad_maximum_fusion.1), channel_id=1, source_target_pairs={{2,0},{4,2},{6,4},{8,6},{10,8},{12,10},{14,12},{16,14},{18,16},{20... | collective-permute-start | bytes 1572872 | tf_op jit(solution)/shard_map/ppermute | solution.py:15
  23.5 11.3 %copy-start.4 = (bf16[2,256,512]{1,2,0:T(8,128)(2,1)}, bf16[2,256,512]{1,2,0:T(8,128)(2,1)S(1)}, u32[]{:S(2)}) copy-start(bf16[2,256,512]{1,2,0:T(8,128)(2,1)S(1)} %collective-permute-done) | copy-start | bytes 1572868
  32.9 3.8 %copy-start.10 = (bf16[1,64,4,4,128]{4,3,2,1,0:T(4,128)(2,1)S(1)}, bf16[1,64,4,4,128]{4,3,2,1,0:T(4,128)(2,1)}, u32[]{:S(2)}) copy-start(bf16[1,64,4,4,128]{4,3,2,1,0:T(4,128)(2,1)} %reshape.470) | copy-start | bytes 786436
  34.8 20.1 %collective-permute-start.2 = (bf16[2,256,512]{1,2,0:T(8,128)(2,1)S(1)}, bf16[2,256,512]{1,2,0:T(8,128)(2,1)}, u32[]{:S(2)}, u32[]{:S(2)}) collective-permute-start(bf16[2,256,512]{1,2,0:T(8,128)(2,1)S(1)} %collective-permute-done), channel_id=1, source_target_pairs={{0,2},{2,4},{4,6},{6,8},{8,10},{10,12},{12,14},{14,16},{16,18},{18... | collective-permute-start | bytes 1572872 | tf_op jit(solution)/shard_map/ppermute | solution.py:15
  37.5 24.5 %collective-permute-start.5 = (bf16[2,256,512]{1,2,0:T(8,128)(2,1)}, bf16[2,256,512]{1,2,0:T(8,128)(2,1)}, u32[]{:S(2)}, u32[]{:S(2)}) collective-permute-start(bf16[2,256,512]{1,2,0:T(8,128)(2,1)} %collective-permute-done.1), channel_id=1, source_target_pairs={{2,0},{4,2},{6,4},{8,6},{10,8},{12,10},{14,12},{16,14},{18,16},{20... | collective-permute-start | bytes 1572872 | tf_op jit(solution)/shard_map/ppermute | solution.py:15
  47.4 9.5 %copy-start.1 = (bf16[2,768,512]{1,2,0:T(8,128)(2,1)S(1)}, bf16[2,768,512]{1,2,0:T(8,128)(2,1)}, u32[]{:S(2)}) copy-start(bf16[2,768,512]{1,2,0:T(8,128)(2,1)} %pad_maximum_fusion) | copy-start | bytes 4718596
  54.9 18.7 %collective-permute-start.3 = (bf16[2,256,512]{1,2,0:T(8,128)(2,1)}, bf16[2,256,512]{1,2,0:T(8,128)(2,1)}, u32[]{:S(2)}, u32[]{:S(2)}) collective-permute-start(bf16[2,256,512]{1,2,0:T(8,128)(2,1)} %collective-permute-done.2), channel_id=1, source_target_pairs={{0,2},{2,4},{4,6},{6,8},{8,10},{10,12},{12,14},{14,16},{16,18},{18... | collective-permute-start | bytes 1572872 | tf_op jit(solution)/shard_map/ppermute | solution.py:15
  57.6 2.6 %copy-start.11 = (pred[256,384]{0,1:T(8,128)(4,1)S(1)}, pred[256,384]{0,1:T(8,128)(4,1)}, u32[]{:S(2)}) copy-start(pred[256,384]{0,1:T(8,128)(4,1)} %fusion.18) | copy-start | bytes 294916
  58.8 16.8 %copy-start.7 = (bf16[2,384,1,4,128]{4,1,3,2,0:T(8,128)(2,1)S(1)}, bf16[2,384,1,4,128]{4,1,3,2,0:T(8,128)(2,1)}, u32[]{:S(2)}) copy-start(bf16[2,384,1,4,128]{4,1,3,2,0:T(8,128)(2,1)} %copy.51) | copy-start | bytes 2359300
  61.9 17.7 %collective-permute-start.6 = (bf16[2,256,512]{1,2,0:T(8,128)(2,1)}, bf16[2,256,512]{1,2,0:T(8,128)(2,1)S(1)}, u32[]{:S(2)}, u32[]{:S(2)}) collective-permute-start(bf16[2,256,512]{1,2,0:T(8,128)(2,1)} %collective-permute-done.5), channel_id=1, source_target_pairs={{2,0},{4,2},{6,4},{8,6},{10,8},{12,10},{14,12},{16,14},{18,16},{20... | collective-permute-start | bytes 1572872 | tf_op jit(solution)/shard_map/ppermute | solution.py:15
  73.7 17.8 %collective-permute-start.4 = (bf16[2,256,512]{1,2,0:T(8,128)(2,1)}, bf16[2,256,512]{1,2,0:T(8,128)(2,1)S(1)}, u32[]{:S(2)}, u32[]{:S(2)}) collective-permute-start(bf16[2,256,512]{1,2,0:T(8,128)(2,1)} %collective-permute-done.3), channel_id=1, source_target_pairs={{0,2},{2,4},{4,6},{6,8},{8,10},{10,12},{12,14},{14,16},{16,18},{18... | collective-permute-start | bytes 1572872 | tf_op jit(solution)/shard_map/ppermute | solution.py:15
  76.9 19.3 %copy-start.5 = (bf16[2,256,512]{1,2,0:T(8,128)(2,1)S(1)}, bf16[2,256,512]{1,2,0:T(8,128)(2,1)}, u32[]{:S(2)}) copy-start(bf16[2,256,512]{1,2,0:T(8,128)(2,1)} %copy-done.4) | copy-start | bytes 1572868
  79.6 22.9 %collective-permute-start.7 = (bf16[2,256,512]{1,2,0:T(8,128)(2,1)S(1)}, bf16[2,256,512]{1,2,0:T(8,128)(2,1)S(1)}, u32[]{:S(2)}, u32[]{:S(2)}) collective-permute-start(bf16[2,256,512]{1,2,0:T(8,128)(2,1)S(1)} %collective-permute-done.6), channel_id=1, source_target_pairs={{2,0},{4,2},{6,4},{8,6},{10,8},{12,10},{14,12},{16,14},{18,16},{20... | collective-permute-start | bytes 1572872 | tf_op jit(solution)/shard_map/ppermute | solution.py:15
  117.8 7.9 %copy-start.9 = (bf16[1,16,16,4,128]{4,3,2,1,0:T(4,128)(2,1)S(1)}, bf16[1,16,16,4,128]{4,3,2,1,0:T(4,128)(2,1)}, u32[]{:S(2)}) copy-start(bf16[1,16,16,4,128]{4,3,2,1,0:T(4,128)(2,1)} %reshape.472) | copy-start | bytes 786436
  117.8 7.9 %copy-start.12 = (pred[16,16,144]{2,1,0:T(8,128)(4,1)S(1)}, pred[16,16,144]{2,1,0:T(8,128)(4,1)}, u32[]{:S(2)}) copy-start(pred[16,16,144]{2,1,0:T(8,128)(4,1)} %and_and_fusion) | copy-start | bytes 110596
  125.7 2.1 %copy-start.2 = (bf16[2,144,16,4,128]{4,1,3,2,0:T(8,128)(2,1)}, bf16[2,144,16,4,128]{4,1,3,2,0:T(8,128)(2,1)S(1)}, u32[]{:S(2)}) copy-start(bf16[2,144,16,4,128]{4,1,3,2,0:T(8,128)(2,1)S(1)} %copy.88) | copy-start | bytes 14155780
  127.8 1.0 copy-start.6
  129.5 3.2 %copy-start.8 = (f32[1,256,4,128]{3,1,2,0:T(8,128)S(1)}, f32[1,256,4,128]{3,1,2,0:T(8,128)}, u32[]{:S(2)}) copy-start(f32[1,256,4,128]{3,1,2,0:T(8,128)} %convolution_bitcast_fusion.1) | copy-start | bytes 1572868
where the time goes:
time: 144 us; the launch traced here: 143 us
  local copies, waits for them, and re-layouts  52.6 us (37%)
  starting transfers between devices  44.4 us (31%)
  waiting for transfers between devices  19.7 us (14%)
  matrix products  10.5 us (7%)
  blocking collectives  7.88 us (5%)
  other arithmetic  7.36 us (5%)
    ppermute x8, starting transfers between devices, from_behind(): lax.ppermute(value, axis, [(source, source + steps) for source in range(f...  44.4 us
    reshape x5, local copies, waits for them, and re-layouts, band_scores(): window_keys.reshape(2, residue_rows + 2 * SIDE_KEY_COUNT, dilation_step,...  22.1 us
    ppermute x8, waiting for transfers between devices, from_behind(): lax.ppermute(value, axis, [(source, source + steps) for source in range(f...  19.7 us
    unnamed x35, local copies, waits for them, and re-layouts  14.3 us
    concatenate x3, local copies, waits for them, and re-layouts, per_device(): extended = jnp.concatenate(far_blocks(stacked_groups, hop_count), axis=1)  10.2 us
    all_to_all x1, blocking collectives, sent_to_all(): lax.all_to_all(jnp.broadcast_to(x[None], (size, *x.shape)), axis, 0, 0, t...  7.88 us
    dot_general x3, matrix products, one_block(): jnp.einsum('rhqk,rhke->rhqe', weights, laid[1], preferred_element_type=jn...  5.4 us
    dot_general x3, matrix products, one_block(): jnp.einsum('rhqe,rhke->rhqk', query_block, laid[0], preferred_element_typ...  3.62 us
  transfers between devices with their start and end apart: 8, of which 6 were waited for; matrix products, arithmetic and copies ran while one was open for 17% of the time, Pallas kernels for 0%

commit v1 on v0

v1 whole, which is shorter than its diff:
```python
import functools
import math

import jax
import jax.numpy as jnp
from jax import lax
from jax.experimental import pallas as pl
from jax.experimental.pallas import tpu as pltpu
from jax.sharding import PartitionSpec as P

HEAD_DIM = 128
SIDE = 64
ROW = 4
SUB = 4
BLK = 16
MESH = pl.DeviceIdType.MESH
BF, F32 = jnp.bfloat16, jnp.float32
NEG = -1e30
COEF = math.log2(math.e) / math.sqrt(HEAD_DIM)
PEERS = (1, 3, 2)


def attend(q, k, v, bias):
    s = lax.dot_general(q, k, (((1,), (1,)), ((), ())), preferred_element_type=F32)
    t = s * COEF + bias
    m = jnp.max(t, axis=1, keepdims=True)
    p = jnp.exp2(t - m)
    l = jnp.sum(p, axis=1, keepdims=True)
    acc = jnp.dot(p.astype(BF), v, preferred_element_type=F32)
    return m, l, acc


def kernel(
    n, heads, q_hbm, k_hbm, v_hbm, w_hbm, out_ref,
    qn, kn, vn, w, xkv, xq, kvres, qres, sret, sstat, ret, rstat,
    nacc, nm, nl, attm, attp, near_bias, mid_bias, far_bias, lead,
    lsem, xs, xr, ys, yr, ns, nr, rs, rr, ts, tr,
):
    sp, tp = lax.axis_index("sp"), lax.axis_index("tp")
    x = lax.rem(sp, ROW)
    base = sp - x
    up = lax.rem(sp + ROW, n)
    down = lax.rem(sp + n - ROW, n)
    right = lax.rem(sp + 1, n)
    left = lax.rem(sp + n - 1, n)
    rows = qn.shape[0]
    piece = rows // ROW

    loads = [
        pltpu.make_async_copy(k_hbm, kn.at[pl.ds(SIDE, rows)], lsem.at[0]),
        pltpu.make_async_copy(v_hbm, vn.at[pl.ds(SIDE, rows)], lsem.at[1]),
        pltpu.make_async_copy(q_hbm, qn, lsem.at[2]),
        pltpu.make_async_copy(w_hbm, w, lsem.at[3]),
    ]
    for copy in loads:
        copy.start()

    def xpeer(k):
        return lax.rem(x + k, ROW)

    barrier = pltpu.get_barrier_semaphore()
    friends = [(base + xpeer(k), tp) for k in PEERS]
    friends += [(up, tp), (down, tp), (right, tp), (left, tp), (sp, 1 - tp)]
    for friend in friends:
        pl.semaphore_signal(barrier, inc=1, device_id=friend, device_id_type=MESH)

    first = (sp < ROW).astype(jnp.int32)
    last = (sp >= n - ROW).astype(jnp.int32)
    start = (sp == 0).astype(jnp.int32)
    end = (sp == n - 1).astype(jnp.int32)

    def iota(shape, dim):
        return lax.broadcasted_iota(jnp.int32, shape, dim)

    r, t = iota((rows, rows), 0), iota((rows, rows), 1)
    order = (r & 15) * 16 + ((r >> 4) & 3) * 4 + (r >> 6)
    perm = jnp.where(t == order, 1.0, 0.0).astype(BF)
    place = (r & 3) * 64 + ((r >> 2) & 3) * 16 + (r >> 4)
    unperm = jnp.where(t == place, 1.0, 0.0).astype(BF)

    loads[0].wait()
    kp = jnp.dot(perm, kn[SIDE : SIDE + rows], preferred_element_type=F32).astype(BF)
    loads[1].wait()
    vp = jnp.dot(perm, vn[SIDE : SIDE + rows], preferred_element_type=F32).astype(BF)

    def cut(a, c, h):
        a = a[c * piece : (c + 1) * piece, h * HEAD_DIM : (h + 1) * HEAD_DIM]
        return a.reshape(SUB, BLK, HEAD_DIM)

    for h in range(heads):
        for c in range(ROW):
            xkv[c, h, 0] = cut(kp, c, h)
            xkv[c, h, 1] = cut(vp, c, h)
    for h in range(heads):
        kvres[h, :, ROW + x] = xkv[x, h]
    loads[2].wait()
    qp = jnp.dot(perm, qn[...], preferred_element_type=F32).astype(BF)
    for h in range(heads):
        for c in range(ROW):
            xq[c, h] = cut(qp, c, h)
    for h in range(heads):
        qres[h, x] = xq[x, h]

    pl.semaphore_wait(barrier, len(friends))

    def remote(src, dst, ssem, rsem, device):
        return pltpu.make_async_remote_copy(
            src_ref=src, dst_ref=dst, send_sem=ssem, recv_sem=rsem,
            device_id=device, device_id_type=MESH,
        )

    def x_kv(h, k):
        c = xpeer(k)
        return remote(
            xkv.at[c, h], kvres.at[h, :, ROW + x], xs.at[h, k, 0], xr.at[h, k, 0], (base + c, tp)
        )

    def x_q(h, k):
        c = xpeer(k)
        return remote(xq.at[c, h], qres.at[h, x], xs.at[h, k, 1], xr.at[h, k, 1], (base + c, tp))

    def y_kv(h, k, way):
        s = xpeer(ROW - k)
        region = 0 if way == 0 else 2 * ROW
        return remote(
            kvres.at[h, :, ROW + s], kvres.at[h, :, region + s],
            ys.at[h, k, way], yr.at[h, k, way], (up if way == 0 else down, tp),
        )

    def near_copies():
        made = []
        for i, a in enumerate((kn, vn)):
            made.append(remote(
                a.at[pl.ds(rows, SIDE)], a.at[pl.ds(0, SIDE)], ns.at[i, 0], nr.at[i, 0], (right, tp)
            ))
            made.append(remote(
                a.at[pl.ds(SIDE, SIDE)], a.at[pl.ds(SIDE + rows, SIDE)],
                ns.at[i, 1], nr.at[i, 1], (left, tp),
            ))
        return made

    for h in range(heads):
        for k in PEERS:
            x_kv(h, k).start()
        for way in (0, 1):
            y_kv(h, 0, way).start()
    halos = near_copies()
    for h in range(heads):
        for k in PEERS:
            x_q(h, k).start()
        if h == 1:
            for copy in halos:
                copy.start()

    iq, ik = iota((2 * SIDE, 4 * SIDE), 0), iota((2 * SIDE, 4 * SIDE), 1)
    band = (ik >= iq) & (ik <= iq + 2 * SIDE)
    near_bias[0] = jnp.where(band & (ik >= start * SIDE), 0.0, NEG)
    near_bias[1] = jnp.where(band & (ik < 4 * SIDE - end * SIDE), 0.0, NEG)
    iq, ik = iota((SIDE, 3 * SIDE), 0), iota((SIDE, 3 * SIDE), 1)
    low, high = first * SIDE, (3 - last) * SIDE
    inside = (ik >= low) & (ik < high)
    far_bias[...] = jnp.where((ik >= iq) & (ik <= iq + 2 * SIDE) & inside, 0.0, NEG)
    wq = (iq & 15) * 4 + (iq >> 4)
    wk = (ik >> 6) * 64 - SIDE + (ik & 15) * 4 + ((ik >> 4) & 3)
    band = (wk - wq <= SIDE) & (wq - wk <= SIDE)
    mid_bias[0] = jnp.where(band & (ik >= low), 0.0, NEG)
    mid_bias[1] = jnp.where(band, 0.0, NEG)
    mid_bias[2] = mid_bias[1]
    mid_bias[3] = jnp.where(band & (ik < high), 0.0, NEG)
    lead[...] = place[:, :HEAD_DIM]

    for h in range(heads):
        for k in PEERS:
            x_kv(h, k).wait_recv()
            for way in (0, 1):
                y_kv(h, k, way).start()

    def near(h):
        cols = slice(h * HEAD_DIM, (h + 1) * HEAD_DIM)
        for b in range(2):
            span = slice(b * 2 * SIDE, (b + 1) * 2 * SIDE)
            keys = slice(b * 2 * SIDE, b * 2 * SIDE + 4 * SIDE)
            m, l, acc = attend(qn[span, cols], kn[keys, cols], vn[keys, cols], near_bias[b])
            nm[h, span] = m
            nl[h, span] = l
            nacc[h, span] = acc

    def give_back(h, k):
        s = xpeer(k)
        return [
            remote(sret.at[h, s], ret.at[h, x], rs.at[h, k, 0], rr.at[h, k, 0], (base + s, tp)),
            remote(sstat.at[h, s], rstat.at[h, x], rs.at[h, k, 1], rr.at[h, k, 1], (base + s, tp)),
        ]

    def residue(h):
        for k in PEERS:
            x_q(h, k).wait_recv()
        for k in range(ROW):
            for way in (0, 1):
                y_kv(h, k, way).wait_recv()
        far = []
        for d in range(SUB):
            q = qres[h, :, d].reshape(SIDE, HEAD_DIM)
            k = kvres[h, 0, :, d].reshape(3 * SIDE, HEAD_DIM)
            v = kvres[h, 1, :, d].reshape(3 * SIDE, HEAD_DIM)
            far.append(attend(q, k, v, far_bias[...]))
        for s in range(ROW):
            q = qres[h, s].reshape(SIDE, HEAD_DIM)
            k = kvres[h, 0, s + 3 : s + 6].reshape(3 * SIDE, HEAD_DIM)
            v = kvres[h, 1, s + 3 : s + 6].reshape(3 * SIDE, HEAD_DIM)
            m1, l1, acc1 = attend(q, k, v, mid_bias[s])
            part = slice(s * BLK, (s + 1) * BLK)
            m2, l2, acc2 = (
                jnp.concatenate([f[i][part] for f in far], axis=0) for i in range(3)
            )
            m = jnp.maximum(m1, m2)
            a1, a2 = jnp.exp2(m1 - m), jnp.exp2(m2 - m)
            l = a1 * l1 + a2 * l2
            inv = 1.0 / l
            sret[h, s] = ((a1 * inv) * acc1 + (a2 * inv) * acc2).astype(BF)
            lse = jnp.broadcast_to(m + jnp.log2(l), (SIDE, HEAD_DIM))
            flat = jnp.transpose(jnp.concatenate([lse, lse], axis=0))
            sstat[h, s] = flat[:8]
        for k in PEERS:
            for copy in give_back(h, k):
                copy.start()
        ret[h, x] = sret[h, x]
        rstat[h, x] = sstat[h, x]

    def tp_copy(h):
        cols = pl.ds(h * HEAD_DIM, HEAD_DIM)
        return remote(attm.at[:, cols], attp.at[:, cols], ts.at[h], tr.at[h], (sp, 1 - tp))

    def combine(h):
        for k in PEERS:
            for copy in give_back(h, k):
                copy.wait_recv()
        got = ret[h].reshape(rows, HEAD_DIM)
        out = jnp.dot(unperm, got, preferred_element_type=F32)
        lane = iota((rows, HEAD_DIM), 1)
        small = iota((1, HEAD_DIM), 1)
        where = lead[...]
        col = jnp.zeros((rows, HEAD_DIM), F32)
        for pair in range(2):
            row = jnp.where(
                small < piece, rstat[h, 2 * pair, 0:1, :], rstat[h, 2 * pair + 1, 0:1, :]
            )
            col = jnp.where(where == lane + pair * HEAD_DIM, row, col)
        lse = jnp.sum(col, axis=1, keepdims=True)
        m0 = nm[h]
        m = jnp.maximum(m0, lse)
        a0, a1 = jnp.exp2(m0 - m), jnp.exp2(lse - m)
        inv = 1.0 / (a0 * nl[h] + a1)
        att = (a0 * inv) * nacc[h] + (a1 * inv) * out
        attm[:, h * HEAD_DIM : (h + 1) * HEAD_DIM] = att.astype(BF)
        tp_copy(h).start()

    residue(0)
    residue(1)
    for copy in halos:
        copy.wait_recv()
    for h in range(heads):
        near(h)
    residue(2)
    combine(0)
    combine(1)
    residue(3)
    combine(2)
    combine(3)

    loads[3].wait()
    depth = heads * HEAD_DIM
    wm = pl.ds(pl.multiple_of(tp * depth, depth), depth)
    wp = pl.ds(pl.multiple_of((1 - tp) * depth, depth), depth)
    mine = jnp.dot(attm[...], w[wm, :], preferred_element_type=F32)
    for h in range(heads):
        tp_copy(h).wait_recv()
    both = mine + jnp.dot(attp[...], w[wp, :], preferred_element_type=F32)
    out_ref[...] = both.astype(BF)

    for h in range(heads):
        for k in PEERS:
            x_kv(h, k).wait_send()
            x_q(h, k).wait_send()
            for copy in give_back(h, k):
                copy.wait_send()
        for k in range(ROW):
            for way in (0, 1):
                y_kv(h, k, way).wait_send()
        tp_copy(h).wait_send()
    for copy in halos:
        copy.wait_send()


def per_device(n, queries, keys, values, w_out):
    rows, columns = queries.shape
    heads = columns // HEAD_DIM
    width = w_out.shape[1]
    vmem = pltpu.VMEM
    dma = pltpu.SemaphoreType.DMA
    return pl.pallas_call(
        functools.partial(kernel, n, heads),
        out_shape=jax.ShapeDtypeStruct((rows, width), BF),
        in_specs=[pl.BlockSpec(memory_space=pl.ANY)] * 4,
        out_specs=pl.BlockSpec(memory_space=pltpu.VMEM),
        scratch_shapes=[
            vmem((rows, columns), BF),
            vmem((rows + 2 * SIDE, columns), BF),
            vmem((rows + 2 * SIDE, columns), BF),
            vmem(w_out.shape, BF),
            vmem((ROW, heads, 2, SUB, BLK, HEAD_DIM), BF),
            vmem((ROW, heads, SUB, BLK, HEAD_DIM), BF),
            vmem((heads, 2, 3 * ROW, SUB, BLK, HEAD_DIM), BF),
            vmem((heads, ROW, SUB, BLK, HEAD_DIM), BF),
            vmem((heads, ROW, SIDE, HEAD_DIM), BF),
            vmem((heads, ROW, 8, HEAD_DIM), F32),
            vmem((heads, ROW, SIDE, HEAD_DIM), BF),
            vmem((heads, ROW, 8, HEAD_DIM), F32),
            vmem((heads, rows, HEAD_DIM), F32),
            vmem((heads, rows, 1), F32),
            vmem((heads, rows, 1), F32),
            vmem((rows, columns), BF),
            vmem((rows, columns), BF),
            vmem((2, 2 * SIDE, 4 * SIDE), F32),
            vmem((ROW, SIDE, 3 * SIDE), F32),
            vmem((SIDE, 3 * SIDE), F32),
            vmem((rows, HEAD_DIM), jnp.int32),
            dma((4,)),
            dma((heads, ROW, 2)),
            dma((heads, ROW, 2)),
            dma((heads, ROW, 2)),
            dma((heads, ROW, 2)),
            dma((2, 2)),
            dma((2, 2)),
            dma((heads, ROW, 2)),
            dma((heads, ROW, 2)),
            dma((heads,)),
            dma((heads,)),
        ],
        compiler_params=pltpu.CompilerParams(collective_id=0, has_side_effects=True),
        name="fused",
    )(queries, keys, values, w_out)


def solution(mesh):
    return jax.shard_map(
        functools.partial(per_device, mesh.shape["sp"]),
        mesh=mesh,
        in_specs=(P("sp", "tp"), P("sp", "tp"), P("sp", "tp"), P(None, "tp")),
        out_specs=P("sp", "tp"),
        check_vma=False,
    )
```

time: 144 us -> 53.5 us (0.37)
  the two profiles are of different devices: /device:TPU:513 before, /device:TPU:1 now
where the time goes in v1:
time: 53.5 us; the launch traced here: 53.3 us
  Pallas kernels  51.5 us (96%)
  local copies, waits for them, and re-layouts  1.87 us (3%)
    pallas_call x1, Pallas kernels, per_device(): pl.pallas_call(functools.partial(kernel, n, heads), out_shape=jax.ShapeDt...  51.5 us
    unnamed x1, local copies, waits for them, and re-layouts  1.87 us

profile of v1, /device:TPU:1, one launch (start us, length us, event | category | flops | bytes accessed | tf_op | source)
XLA Modules:
  0.0 53.3 jit_solution(6222579615803713105)
XLA Ops:
  0.0 51.5 %fused.1 = bf16[256,1024]{1,0:T(8,128)(2,1)} custom-call(bf16[256,512]{1,0:T(8,128)(2,1)} %q_hbm.1, bf16[256,512]{1,0:T(8,128)(2,1)} %k_hbm.1, bf16[256,512]{1,0:T(8,128)(2,1)} %v_hbm.1, bf16[1024,1024]{1,0:T(8,128)(2,1)} %w_hbm.1), custom_call_target="tpu_custom_call" | custom-call | tf_op jit(solution)/shard_map/fused/pallas_call | solution.py:301
  51.5 1.9 %copy.6 = bf16[256,1024]{1,0:T(8,128)(2,1)} copy(bf16[256,1024]{1,0:T(8,128)(2,1)} %fused.1) | data formatting | bytes 1048576

commit v2 on v1

v2 whole, which is shorter than its diff:
```python
import functools
import math

import jax
import jax.numpy as jnp
from jax import lax
from jax.experimental import pallas as pl
from jax.experimental.pallas import tpu as pltpu
from jax.sharding import PartitionSpec as P

HEAD_DIM = 128
SIDE = 64
ROW = 4
SUB = 4
BLK = 16
MESH = pl.DeviceIdType.MESH
BF, F32 = jnp.bfloat16, jnp.float32
NEG = -1e30
COEF = math.log2(math.e) / math.sqrt(HEAD_DIM)
PEERS = (1, 3, 2)


def attend(q, k, v, bias):
    s = lax.dot_general(q, k, (((1,), (1,)), ((), ())), preferred_element_type=F32)
    t = s * COEF + bias
    m = jnp.max(t, axis=1, keepdims=True)
    p = jnp.exp2(t - m)
    l = jnp.sum(p, axis=1, keepdims=True)
    acc = jnp.dot(p.astype(BF), v, preferred_element_type=F32)
    return m, l, acc


def kernel(
    n, heads, q_hbm, k_hbm, v_hbm, out_ref,
    qn, kn, vn, xkv, xq, kvres, qres, sret, sstat, ret, rstat,
    nacc, nm, nl, near_bias, mid_bias, far_bias, lead,
    lsem, xs, xr, ys, yr, ns, nr, rs, rr, ts, tr,
):
    sp, tp = lax.axis_index("sp"), lax.axis_index("tp")
    x = lax.rem(sp, ROW)
    base = sp - x
    up = lax.rem(sp + ROW, n)
    down = lax.rem(sp + n - ROW, n)
    right = lax.rem(sp + 1, n)
    left = lax.rem(sp + n - 1, n)
    rows = qn.shape[0]
    piece = rows // ROW

    loads = [
        pltpu.make_async_copy(k_hbm, kn.at[pl.ds(SIDE, rows)], lsem.at[0]),
        pltpu.make_async_copy(v_hbm, vn.at[pl.ds(SIDE, rows)], lsem.at[1]),
        pltpu.make_async_copy(q_hbm, qn, lsem.at[2]),
    ]
    for copy in loads:
        copy.start()

    def xpeer(k):
        return lax.rem(x + k, ROW)

    first = (sp < ROW).astype(jnp.int32)
    last = (sp >= n - ROW).astype(jnp.int32)
    start = (sp == 0).astype(jnp.int32)
    end = (sp == n - 1).astype(jnp.int32)
    to_up, to_down, to_right, to_left = sp < n - ROW, sp >= ROW, sp < n - 1, sp >= 1

    barrier = pltpu.get_barrier_semaphore()

    def greet(friend):
        pl.semaphore_signal(barrier, inc=1, device_id=friend, device_id_type=MESH)

    for k in PEERS:
        greet((base + xpeer(k), tp))
    greet((sp, 1 - tp))
    pl.when(to_up)(lambda: greet((up, tp)))
    pl.when(to_down)(lambda: greet((down, tp)))
    pl.when(to_right)(lambda: greet((right, tp)))
    pl.when(to_left)(lambda: greet((left, tp)))

    def iota(shape, dim):
        return lax.broadcasted_iota(jnp.int32, shape, dim)

    r, t = iota((rows, rows), 0), iota((rows, rows), 1)
    order = (r & 15) * 16 + ((r >> 4) & 3) * 4 + (r >> 6)
    perm = jnp.where(t == order, 1.0, 0.0).astype(BF)
    place = (r & 3) * 64 + ((r >> 2) & 3) * 16 + (r >> 4)
    unperm = jnp.where(t == place, 1.0, 0.0).astype(BF)

    loads[0].wait()
    kp = jnp.dot(perm, kn[SIDE : SIDE + rows], preferred_element_type=F32).astype(BF)
    loads[1].wait()
    vp = jnp.dot(perm, vn[SIDE : SIDE + rows], preferred_element_type=F32).astype(BF)

    def cut(a, c, h):
        a = a[c * piece : (c + 1) * piece, h * HEAD_DIM : (h + 1) * HEAD_DIM]
        return a.reshape(SUB, BLK, HEAD_DIM)

    for h in range(heads):
        for c in range(ROW):
            xkv[c, h, 0] = cut(kp, c, h)
            xkv[c, h, 1] = cut(vp, c, h)

    pl.semaphore_wait(barrier, 2 * ROW - first - last - start - end)

    def remote(src, dst, ssem, rsem, device):
        return pltpu.make_async_remote_copy(
            src_ref=src, dst_ref=dst, send_sem=ssem, recv_sem=rsem,
            device_id=device, device_id_type=MESH,
        )

    def x_kv(h, k):
        c = xpeer(k)
        return remote(
            xkv.at[c, h], kvres.at[h, ROW + x], xs.at[h, k, 0], xr.at[h, k, 0], (base + c, tp)
        )

    def x_q(h, k):
        c = xpeer(k)
        return remote(xq.at[c, h], qres.at[h, x], xs.at[h, k, 1], xr.at[h, k, 1], (base + c, tp))

    def y_kv(h, k, way):
        s = xpeer(ROW - k)
        region = 0 if way == 0 else 2 * ROW
        return remote(
            xkv.at[x, h] if k == 0 else kvres.at[h, ROW + s], kvres.at[h, region + s],
            ys.at[h, k, way], yr.at[h, k, way], (up if way == 0 else down, tp),
        )

    def y_each(act, pairs, sides):
        for way, side in enumerate(sides):
            @pl.when(side)
            def _():
                for h, k in pairs:
                    getattr(y_kv(h, k, way), act)()

    def halo(act, sides):
        for way, side in enumerate(sides):
            @pl.when(side)
            def _():
                for i, a in enumerate((kn, vn)):
                    if way == 0:
                        src, dst, who = pl.ds(rows, SIDE), pl.ds(0, SIDE), right
                    else:
                        src, dst, who = pl.ds(SIDE, SIDE), pl.ds(SIDE + rows, SIDE), left
                    copy = remote(a.at[src], a.at[dst], ns.at[i, way], nr.at[i, way], (who, tp))
                    getattr(copy, act)()

    y_out, y_in = (to_up, to_down), (to_down, to_up)
    halo_out, halo_in = (to_right, to_left), (to_left, to_right)

    for h in range(heads):
        for k in PEERS:
            x_kv(h, k).start()
    y_each("start", [(h, 0) for h in range(heads)], y_out)
    loads[2].wait()
    qp = jnp.dot(perm, qn[...], preferred_element_type=F32).astype(BF)
    for h in range(heads):
        for c in range(ROW):
            xq[c, h] = cut(qp, c, h)
    for h in range(heads):
        for k in PEERS:
            x_q(h, k).start()
    halo("start", halo_out)
    for h in range(heads):
        kvres[h, ROW + x] = xkv[x, h]
        qres[h, x] = xq[x, h]

    blank = jnp.zeros((heads, ROW, 2, SUB, BLK, HEAD_DIM), BF)
    edge = jnp.zeros((SIDE, heads * HEAD_DIM), BF)

    @pl.when(sp < ROW)
    def _():
        kvres[:, :ROW] = blank

    @pl.when(sp >= n - ROW)
    def _():
        kvres[:, 2 * ROW :] = blank

    @pl.when(sp == 0)
    def _():
        kn[:SIDE] = edge
        vn[:SIDE] = edge

    @pl.when(sp == n - 1)
    def _():
        kn[SIDE + rows :] = edge
        vn[SIDE + rows :] = edge

    iq, ik = iota((2 * SIDE, 4 * SIDE), 0), iota((2 * SIDE, 4 * SIDE), 1)
    band = (ik >= iq) & (ik <= iq + 2 * SIDE)
    near_bias[0] = jnp.where(band & (ik >= start * SIDE), 0.0, NEG)
    near_bias[1] = jnp.where(band & (ik < 4 * SIDE - end * SIDE), 0.0, NEG)
    low, high = first * SIDE, (4 - last) * SIDE
    wq = (iq >> 6) * 64 + (iq & 15) * 4 + ((iq >> 4) & 3)
    wk = (ik >> 6) * 64 - SIDE + (ik & 15) * 4 + ((ik >> 4) & 3)
    band = (wk - wq <= SIDE) & (wq - wk <= SIDE)
    mid_bias[0] = jnp.where(band & (ik >= low), 0.0, NEG)
    mid_bias[1] = jnp.where(band & (ik < high), 0.0, NEG)
    iq, ik = iota((2 * SIDE, 6 * SIDE), 0), iota((2 * SIDE, 6 * SIDE), 1)
    vq = (iq >> 5) * BLK + (iq & 15)
    vk = (ik >> 5) * BLK + (ik & 15)
    band = (vk >= vq) & (vk <= vq + 2 * SIDE) & ((iq & 16) == (ik & 16))
    band = band & (vk >= first * SIDE) & (vk < (3 - last) * SIDE)
    far_bias[...] = jnp.where(band, 0.0, NEG)
    lead[...] = place[:, :HEAD_DIM]

    for h in range(heads):
        for k in PEERS:
            x_kv(h, k).wait_recv()
            y_each("start", [(h, k)], y_out)

    def near(h):
        cols = slice(h * HEAD_DIM, (h + 1) * HEAD_DIM)
        for b in range(2):
            span = slice(b * 2 * SIDE, (b + 1) * 2 * SIDE)
            keys = slice(b * 2 * SIDE, b * 2 * SIDE + 4 * SIDE)
            m, l, acc = attend(qn[span, cols], kn[keys, cols], vn[keys, cols], near_bias[b])
            nm[h, span] = m
            nl[h, span] = l
            nacc[h, span] = acc

    def give_back(h, k):
        s = xpeer(k)
        return [
            remote(sret.at[h, s], ret.at[h, x], rs.at[h, k, 0], rr.at[h, k, 0], (base + s, tp)),
            remote(sstat.at[h, s], rstat.at[h, x], rs.at[h, k, 1], rr.at[h, k, 1], (base + s, tp)),
        ]

    def residue(h):
        for k in PEERS:
            x_q(h, k).wait_recv()
        y_each("wait_recv", [(h, k) for k in range(ROW)], y_in)
        far, mid = [], []
        for e in range(2):
            two = slice(2 * e, 2 * e + 2)
            q = qres[h, :, two].reshape(2 * SIDE, HEAD_DIM)
            k = kvres[h, :, 0, two].reshape(6 * SIDE, HEAD_DIM)
            v = kvres[h, :, 1, two].reshape(6 * SIDE, HEAD_DIM)
            far.append(attend(q, k, v, far_bias[...]))
            q = qres[h, two].reshape(2 * SIDE, HEAD_DIM)
            k = kvres[h, 2 * e + 3 : 2 * e + 7, 0].reshape(4 * SIDE, HEAD_DIM)
            v = kvres[h, 2 * e + 3 : 2 * e + 7, 1].reshape(4 * SIDE, HEAD_DIM)
            mid.append(attend(q, k, v, mid_bias[e]))
        for s in range(ROW):
            part = slice(s % 2 * SIDE, (s % 2 + 1) * SIDE)
            m1, l1, acc1 = (mid[s // 2][i][part] for i in range(3))
            part = slice(s * 2 * BLK, (s + 1) * 2 * BLK)
            m2, l2, acc2 = (
                jnp.concatenate([f[i][part] for f in far], axis=0) for i in range(3)
            )
            m = jnp.maximum(m1, m2)
            a1, a2 = jnp.exp2(m1 - m), jnp.exp2(m2 - m)
            l = a1 * l1 + a2 * l2
            inv = 1.0 / l
            sret[h, s] = ((a1 * inv) * acc1 + (a2 * inv) * acc2).astype(BF)
            lse = jnp.broadcast_to(m + jnp.log2(l), (SIDE, HEAD_DIM))
            flat = jnp.transpose(jnp.concatenate([lse, lse], axis=0))
            sstat[h, s] = flat[:1]
        for k in PEERS:
            for copy in give_back(h, k):
                copy.start()
        ret[h, x] = sret[h, x]
        rstat[h, x] = sstat[h, x]

    def columns(h, side):
        return pl.ds(pl.multiple_of((side * heads + h) * HEAD_DIM, HEAD_DIM), HEAD_DIM)

    def tp_copy(h):
        mine = out_ref.at[:, columns(h, tp)]
        return remote(mine, mine, ts.at[h], tr.at[h], (sp, 1 - tp))

    def combine(h):
        for k in PEERS:
            for copy in give_back(h, k):
                copy.wait_recv()
        got = ret[h].reshape(rows, HEAD_DIM)
        out = jnp.dot(unperm, got, preferred_element_type=F32)
        lane = iota((rows, HEAD_DIM), 1)
        small = iota((1, HEAD_DIM), 1)
        where = lead[...]
        col = jnp.zeros((rows, HEAD_DIM), F32)
        for pair in range(2):
            row = jnp.where(
                small < piece, rstat[h, 2 * pair], rstat[h, 2 * pair + 1]
            )
            col = jnp.where(where == lane + pair * HEAD_DIM, row, col)
        lse = jnp.sum(col, axis=1, keepdims=True)
        m0 = nm[h]
        m = jnp.maximum(m0, lse)
        a0, a1 = jnp.exp2(m0 - m), jnp.exp2(lse - m)
        inv = 1.0 / (a0 * nl[h] + a1)
        att = (a0 * inv) * nacc[h] + (a1 * inv) * out
        out_ref[:, columns(h, tp)] = att.astype(BF)
        tp_copy(h).start()

    for h in range(heads):
        residue(h)
    halo("wait_recv", halo_in)
    for h in range(heads):
        near(h)
    for h in range(heads):
        combine(h)
    for h in range(heads):
        tp_copy(h).wait_recv()

    for h in range(heads):
        for k in PEERS:
            x_kv(h, k).wait_send()
            x_q(h, k).wait_send()
            for copy in give_back(h, k):
                copy.wait_send()
        y_each("wait_send", [(h, k) for k in range(ROW)], y_out)
        tp_copy(h).wait_send()
    halo("wait_send", halo_out)


def per_device(n, queries, keys, values, w_out):
    rows, columns = queries.shape
    heads = columns // HEAD_DIM
    vmem = pltpu.VMEM
    dma = pltpu.SemaphoreType.DMA
    attended = pl.pallas_call(
        functools.partial(kernel, n, heads),
        out_shape=jax.ShapeDtypeStruct((rows, 2 * columns), BF),
        in_specs=[pl.BlockSpec(memory_space=pl.ANY)] * 3,
        out_specs=pl.BlockSpec(memory_space=pltpu.VMEM),
        scratch_shapes=[
            vmem((rows, columns), BF),
            vmem((rows + 2 * SIDE, columns), BF),
            vmem((rows + 2 * SIDE, columns), BF),
            vmem((ROW, heads, 2, SUB, BLK, HEAD_DIM), BF),
            vmem((ROW, heads, SUB, BLK, HEAD_DIM), BF),
            vmem((heads, 3 * ROW, 2, SUB, BLK, HEAD_DIM), BF),
            vmem((heads, ROW, SUB, BLK, HEAD_DIM), BF),
            vmem((heads, ROW, SIDE, HEAD_DIM), BF),
            vmem((heads, ROW, 1, HEAD_DIM), F32),
            vmem((heads, ROW, SIDE, HEAD_DIM), BF),
            vmem((heads, ROW, 1, HEAD_DIM), F32),
            vmem((heads, rows, HEAD_DIM), F32),
            vmem((heads, rows, 1), F32),
            vmem((heads, rows, 1), F32),
            vmem((2, 2 * SIDE, 4 * SIDE), F32),
            vmem((2, 2 * SIDE, 4 * SIDE), F32),
            vmem((2 * SIDE, 6 * SIDE), F32),
            vmem((rows, HEAD_DIM), jnp.int32),
            dma((3,)),
            dma((heads, ROW, 2)),
            dma((heads, ROW, 2)),
            dma((heads, ROW, 2)),
            dma((heads, ROW, 2)),
            dma((2, 2)),
            dma((2, 2)),
            dma((heads, ROW, 2)),
            dma((heads, ROW, 2)),
            dma((heads,)),
            dma((heads,)),
        ],
        compiler_params=pltpu.CompilerParams(
            collective_id=0, has_side_effects=True, vmem_limit_bytes=20 * 1024 * 1024
        ),
        name="fused",
    )(queries, keys, values)
    return jnp.dot(attended, w_out, preferred_element_type=F32).astype(BF)


def solution(mesh):
    return jax.shard_map(
        functools.partial(per_device, mesh.shape["sp"]),
        mesh=mesh,
        in_specs=(P("sp", "tp"), P("sp", "tp"), P("sp", "tp"), P(None, "tp")),
        out_specs=P("sp", "tp"),
        check_vma=False,
    )
```

time: 53.5 us -> 38.8 us (0.73)
  Pallas kernels: 51.5 us -> 33.8 us
  matrix products: 0 us -> 1.51 us
  local copies, waits for them, and re-layouts: 1.87 us -> 3 us
    pallas_call x1, Pallas kernels: 51.5 us -> 33.8 us  [per_device(): pl.pallas_call(functools.partial(kernel, n, heads), out_shape=jax.ShapeDt...]
    dot_general x0 -> x1, matrix products: none -> 1.51 us  [per_device(): return jnp.dot(attended, w_out, preferred_element_type=F32).astype(BF)]
    unnamed x1 -> x8, local copies, waits for them, and re-layouts: 1.87 us -> 3 us
where the time goes in v2:
time: 38.8 us; the launch traced here: 38.4 us
  Pallas kernels  33.8 us (87%)
  local copies, waits for them, and re-layouts  3 us (8%)
  matrix products  1.51 us (4%)
    pallas_call x1, Pallas kernels, per_device(): pl.pallas_call(functools.partial(kernel, n, heads), out_shape=jax.ShapeDt...  33.8 us
    unnamed x8, local copies, waits for them, and re-layouts  3 us
    dot_general x1, matrix products, per_device(): return jnp.dot(attended, w_out, preferred_element_type=F32).astype(BF)  1.51 us

profile of v2, /device:TPU:1, one launch (start us, length us, event | category | flops | bytes accessed | tf_op | source)
XLA Modules:
  0.0 38.4 jit_solution(11105553550323978835)
XLA Ops:
  0.0 0.0 copy-start
  0.0 0.0 copy-start.1
  0.0 1.1 %copy-done.1 = bf16[256,512]{1,0:T(8,128)(2,1)S(1)} copy-done((bf16[256,512]{1,0:T(8,128)(2,1)S(1)}, bf16[256,512]{1,0:T(8,128)(2,1)}, u32[]{:S(2)}) %copy-start.1) | copy-done | bytes 262168
  1.1 0.0 copy-start.2
  1.1 0.9 %copy-done.2 = bf16[256,512]{1,0:T(8,128)(2,1)S(1)} copy-done((bf16[256,512]{1,0:T(8,128)(2,1)S(1)}, bf16[256,512]{1,0:T(8,128)(2,1)}, u32[]{:S(2)}) %copy-start.2) | copy-done | bytes 262168
  2.1 0.0 copy-start.3
  2.1 0.9 %copy-done.3 = bf16[256,512]{1,0:T(8,128)(2,1)S(1)} copy-done((bf16[256,512]{1,0:T(8,128)(2,1)S(1)}, bf16[256,512]{1,0:T(8,128)(2,1)}, u32[]{:S(2)}) %copy-start.3) | copy-done | bytes 262168
  3.0 33.8 %fused.1 = bf16[256,1024]{1,0:T(8,128)(2,1)S(1)} custom-call(bf16[256,512]{1,0:T(8,128)(2,1)S(1)} %copy-done.1, bf16[256,512]{1,0:T(8,128)(2,1)S(1)} %copy-done.2, bf16[256,512]{1,0:T(8,128)(2,1)S(1)} %copy-done.3), custom_call_target="tpu_custom_call" | custom-call | tf_op jit(solution)/shard_map/fused/pallas_call | solution.py:321
  36.8 0.0 copy-done
  36.8 1.5 %convolution_convert_fusion = bf16[256,1024]{1,0:T(8,128)(2,1)} fusion(bf16[256,1024]{1,0:T(8,128)(2,1)S(1)} %fused.1, bf16[1024,1024]{1,0:T(8,128)(2,1)S(1)} %copy-done), kind=kOutput, calls=%fused_computation | convolution fusion | flops 537133056 | bytes 3145728 | tf_op jit(solution)/shard_map/dot_general | solution.py:362
Async XLA Ops:
  0.0 36.8 %copy-start = (bf16[1024,1024]{1,0:T(8,128)(2,1)S(1)}, bf16[1024,1024]{1,0:T(8,128)(2,1)}, u32[]{:S(2)}) copy-start(bf16[1024,1024]{1,0:T(8,128)(2,1)} %param.7) | copy-start | bytes 6291460
  0.0 1.1 %copy-start.1 = (bf16[256,512]{1,0:T(8,128)(2,1)S(1)}, bf16[256,512]{1,0:T(8,128)(2,1)}, u32[]{:S(2)}) copy-start(bf16[256,512]{1,0:T(8,128)(2,1)} %q_hbm.1) | copy-start | bytes 786436
  1.1 0.9 %copy-start.2 = (bf16[256,512]{1,0:T(8,128)(2,1)S(1)}, bf16[256,512]{1,0:T(8,128)(2,1)}, u32[]{:S(2)}) copy-start(bf16[256,512]{1,0:T(8,128)(2,1)} %k_hbm.1) | copy-start | bytes 786436
  2.1 0.9 %copy-start.3 = (bf16[256,512]{1,0:T(8,128)(2,1)S(1)}, bf16[256,512]{1,0:T(8,128)(2,1)}, u32[]{:S(2)}) copy-start(bf16[256,512]{1,0:T(8,128)(2,1)} %v_hbm.1) | copy-start | bytes 786436

commit v3 on v2

--- a/solution.py
+++ b/solution.py
@@ -14,6 +14,7 @@
 SUB = 4
 BLK = 16
 MESH = pl.DeviceIdType.MESH
+scope = jax.named_scope
 BF, F32 = jnp.bfloat16, jnp.float32
 NEG = -1e30
 COEF = math.log2(math.e) / math.sqrt(HEAD_DIM)
@@ -34,7 +35,7 @@
     n, heads, q_hbm, k_hbm, v_hbm, out_ref,
     qn, kn, vn, xkv, xq, kvres, qres, sret, sstat, ret, rstat,
     nacc, nm, nl, near_bias, mid_bias, far_bias, lead,
-    lsem, xs, xr, ys, yr, ns, nr, rs, rr, ts, tr,
+    lsem, xs, xr, qr, ys, yr, ns, nr, rs, rr, ts,
 ):
     sp, tp = lax.axis_index("sp"), lax.axis_index("tp")
     x = lax.rem(sp, ROW)
@@ -85,9 +86,11 @@
     place = (r & 3) * 64 + ((r >> 2) & 3) * 16 + (r >> 4)
     unperm = jnp.where(t == place, 1.0, 0.0).astype(BF)
 
-    loads[0].wait()
+    with scope("load_k"):
+        loads[0].wait()
     kp = jnp.dot(perm, kn[SIDE : SIDE + rows], preferred_element_type=F32).astype(BF)
-    loads[1].wait()
+    with scope("load_v"):
+        loads[1].wait()
     vp = jnp.dot(perm, vn[SIDE : SIDE + rows], preferred_element_type=F32).astype(BF)
 
     def cut(a, c, h):
@@ -99,7 +102,8 @@
             xkv[c, h, 0] = cut(kp, c, h)
             xkv[c, h, 1] = cut(vp, c, h)
 
-    pl.semaphore_wait(barrier, 2 * ROW - first - last - start - end)
+    with scope("barrier"):
+        pl.semaphore_wait(barrier, 2 * ROW - first - last - start - end)
 
     def remote(src, dst, ssem, rsem, device):
         return pltpu.make_async_remote_copy(
@@ -110,39 +114,53 @@
     def x_kv(h, k):
         c = xpeer(k)
         return remote(
-            xkv.at[c, h], kvres.at[h, ROW + x], xs.at[h, k, 0], xr.at[h, k, 0], (base + c, tp)
+            xkv.at[c, h], kvres.at[h, ROW + x], xs.at[0], xr.at[h, k - 1], (base + c, tp)
         )
 
     def x_q(h, k):
         c = xpeer(k)
-        return remote(xq.at[c, h], qres.at[h, x], xs.at[h, k, 1], xr.at[h, k, 1], (base + c, tp))
+        return remote(xq.at[c, h], qres.at[h, x], xs.at[1], qr.at[h], (base + c, tp))
 
     def y_kv(h, k, way):
         s = xpeer(ROW - k)
         region = 0 if way == 0 else 2 * ROW
         return remote(
             xkv.at[x, h] if k == 0 else kvres.at[h, ROW + s], kvres.at[h, region + s],
-            ys.at[h, k, way], yr.at[h, k, way], (up if way == 0 else down, tp),
+            ys.at[way], yr.at[h, way], (up if way == 0 else down, tp),
         )
 
-    def y_each(act, pairs, sides):
-        for way, side in enumerate(sides):
+    def taken(ref, sem):
+        remote(ref, ref, sem, sem, (sp, 1 - tp)).wait_recv()
+
+    def y_send(pairs):
+        for way, side in enumerate(y_out):
             @pl.when(side)
             def _():
                 for h, k in pairs:
-                    getattr(y_kv(h, k, way), act)()
-
-    def halo(act, sides):
-        for way, side in enumerate(sides):
+                    y_kv(h, k, way).start()
+
+    def y_wait(h):
+        for way, side in enumerate(y_in):
             @pl.when(side)
             def _():
-                for i, a in enumerate((kn, vn)):
+                taken(kvres.at[h, pl.ds(0, ROW)], yr.at[h, way])
+
+    def halo_send():
+        for way, side in enumerate(halo_out):
+            @pl.when(side)
+            def _():
+                for a in (kn, vn):
                     if way == 0:
                         src, dst, who = pl.ds(rows, SIDE), pl.ds(0, SIDE), right
                     else:
                         src, dst, who = pl.ds(SIDE, SIDE), pl.ds(SIDE + rows, SIDE), left
-                    copy = remote(a.at[src], a.at[dst], ns.at[i, way], nr.at[i, way], (who, tp))
-                    getattr(copy, act)()
+                    remote(a.at[src], a.at[dst], ns.at[way], nr.at[way], (who, tp)).start()
+
+    def halo_wait(sems, sides):
+        for way, side in enumerate(sides):
+            @pl.when(side)
+            def _():
+                taken(kn.at[pl.ds(0, 2 * SIDE)], sems.at[way])
 
     y_out, y_in = (to_up, to_down), (to_down, to_up)
     halo_out, halo_in = (to_right, to_left), (to_left, to_right)
@@ -150,8 +168,9 @@
     for h in range(heads):
         for k in PEERS:
             x_kv(h, k).start()
-    y_each("start", [(h, 0) for h in range(heads)], y_out)
-    loads[2].wait()
+    y_send([(h, 0) for h in range(heads)])
+    with scope("load_q"):
+        loads[2].wait()
     qp = jnp.dot(perm, qn[...], preferred_element_type=F32).astype(BF)
     for h in range(heads):
         for c in range(ROW):
@@ -159,7 +178,6 @@
     for h in range(heads):
         for k in PEERS:
             x_q(h, k).start()
-    halo("start", halo_out)
     for h in range(heads):
         kvres[h, ROW + x] = xkv[x, h]
         qres[h, x] = xq[x, h]
@@ -203,10 +221,11 @@
     far_bias[...] = jnp.where(band, 0.0, NEG)
     lead[...] = place[:, :HEAD_DIM]
 
-    for h in range(heads):
+    def relay(h):
         for k in PEERS:
-            x_kv(h, k).wait_recv()
-            y_each("start", [(h, k)], y_out)
+            with scope(f"relay_{h}_{k}"):
+                x_kv(h, k).wait_recv()
+            y_send([(h, k)])
 
     def near(h):
         cols = slice(h * HEAD_DIM, (h + 1) * HEAD_DIM)
@@ -221,14 +240,15 @@
     def give_back(h, k):
         s = xpeer(k)
         return [
-            remote(sret.at[h, s], ret.at[h, x], rs.at[h, k, 0], rr.at[h, k, 0], (base + s, tp)),
-            remote(sstat.at[h, s], rstat.at[h, x], rs.at[h, k, 1], rr.at[h, k, 1], (base + s, tp)),
+            remote(sret.at[h, s], ret.at[h, x], rs.at[0], rr.at[h, 0], (base + s, tp)),
+            remote(sstat.at[h, s], rstat.at[h, x], rs.at[1], rr.at[h, 1], (base + s, tp)),
         ]
 
     def residue(h):
-        for k in PEERS:
-            x_q(h, k).wait_recv()
-        y_each("wait_recv", [(h, k) for k in range(ROW)], y_in)
+        with scope(f"wait_q_{h}"):
+            taken(qres.at[h, pl.ds(0, ROW - 1)], qr.at[h])
+        with scope(f"wait_y_{h}"):
+            y_wait(h)
         far, mid = [], []
         for e in range(2):
             two = slice(2 * e, 2 * e + 2)
@@ -266,12 +286,12 @@
 
     def tp_copy(h):
         mine = out_ref.at[:, columns(h, tp)]
-        return remote(mine, mine, ts.at[h], tr.at[h], (sp, 1 - tp))
+        return remote(mine, mine, ts.at[0], ts.at[1], (sp, 1 - tp))
 
     def combine(h):
-        for k in PEERS:
-            for copy in give_back(h, k):
-                copy.wait_recv()
+        with scope(f"wait_back_{h}"):
+            taken(ret.at[h, pl.ds(0, ROW - 1)], rr.at[h, 0])
+            taken(rstat.at[h, pl.ds(0, ROW - 1)], rr.at[h, 1])
         got = ret[h].reshape(rows, HEAD_DIM)
         out = jnp.dot(unperm, got, preferred_element_type=F32)
         lane = iota((rows, HEAD_DIM), 1)
@@ -292,25 +312,35 @@
         out_ref[:, columns(h, tp)] = att.astype(BF)
         tp_copy(h).start()
 
-    for h in range(heads):
-        residue(h)
-    halo("wait_recv", halo_in)
+    relay(0)
+    relay(1)
+    relay(2)
+    residue(0)
+    relay(3)
+    halo_send()
+    residue(1)
+    residue(2)
+    residue(3)
+    with scope("wait_halo"):
+        halo_wait(nr, halo_in)
     for h in range(heads):
         near(h)
     for h in range(heads):
         combine(h)
-    for h in range(heads):
-        tp_copy(h).wait_recv()
-
-    for h in range(heads):
-        for k in PEERS:
-            x_kv(h, k).wait_send()
-            x_q(h, k).wait_send()
-            for copy in give_back(h, k):
-                copy.wait_send()
-        y_each("wait_send", [(h, k) for k in range(ROW)], y_out)
-        tp_copy(h).wait_send()
-    halo("wait_send", halo_out)
+
+    with scope("send_waits"):
+        taken(xkv.at[pl.ds(0, ROW - 1)], xs.at[0])
+        taken(xq.at[pl.ds(0, ROW - 1)], xs.at[1])
+        for way, side in enumerate(y_out):
+            @pl.when(side)
+            def _():
+                taken(xkv, ys.at[way])
+        halo_wait(ns, halo_out)
+        taken(sret.at[:, pl.ds(0, ROW - 1)], rs.at[0])
+        taken(sstat.at[:, pl.ds(0, ROW - 1)], rs.at[1])
+    with scope("wait_tp"):
+        taken(qn, ts.at[1])
+        taken(qn, ts.at[0])
 
 
 def per_device(n, queries, keys, values, w_out):
@@ -321,7 +351,7 @@
     attended = pl.pallas_call(
         functools.partial(kernel, n, heads),
         out_shape=jax.ShapeDtypeStruct((rows, 2 * columns), BF),
-        in_specs=[pl.BlockSpec(memory_space=pl.ANY)] * 3,
+        in_specs=[pl.BlockSpec(memory_space=pltpu.HBM)] * 3,
         out_specs=pl.BlockSpec(memory_space=pltpu.VMEM),
         scratch_shapes=[
             vmem((rows, columns), BF),
@@ -343,22 +373,22 @@
             vmem((2 * SIDE, 6 * SIDE), F32),
             vmem((rows, HEAD_DIM), jnp.int32),
             dma((3,)),
-            dma((heads, ROW, 2)),
-            dma((heads, ROW, 2)),
-            dma((heads, ROW, 2)),
-            dma((heads, ROW, 2)),
-            dma((2, 2)),
-            dma((2, 2)),
-            dma((heads, ROW, 2)),
-            dma((heads, ROW, 2)),
+            dma((2,)),
+            dma((heads, ROW - 1)),
             dma((heads,)),
-            dma((heads,)),
+            dma((2,)),
+            dma((heads, 2)),
+            dma((2,)),
+            dma((2,)),
+            dma((2,)),
+            dma((heads, 2)),
+            dma((2,)),
         ],
         compiler_params=pltpu.CompilerParams(
             collective_id=0, has_side_effects=True, vmem_limit_bytes=20 * 1024 * 1024
         ),
         name="fused",
-    )(queries, keys, values)
+    )(*(pltpu.with_memory_space_constraint(a, pltpu.HBM) for a in (queries, keys, values)))
     return jnp.dot(attended, w_out, preferred_element_type=F32).astype(BF)
 
 

time: 38.8 us -> 34.7 us (0.89)
  local copies, waits for them, and re-layouts: 3 us -> 0.01 us
  Pallas kernels: 33.8 us -> 33 us
    unnamed x8 -> x2, local copies, waits for them, and re-layouts: 3 us -> 0.01 us
    pallas_call x1, Pallas kernels: 33.8 us -> 33 us  [per_device(): pl.pallas_call(functools.partial(kernel, n, heads), out_shape=jax.ShapeDt...]
where the time goes in v3:
time: 34.7 us; the launch traced here: 34.5 us
  Pallas kernels  33 us (95%)
  matrix products  1.51 us (4%)
    pallas_call x1, Pallas kernels, per_device(): pl.pallas_call(functools.partial(kernel, n, heads), out_shape=jax.ShapeDt...  33 us
    dot_general x1, matrix products, per_device(): return jnp.dot(attended, w_out, preferred_element_type=F32).astype(BF)  1.51 us

profile of v3, /device:TPU:1, one launch (start us, length us, event | category | flops | bytes accessed | tf_op | source)
XLA Modules:
  0.0 34.5 jit_solution(14474289615209927035)
XLA Ops:
  0.0 0.0 copy-start
  0.0 33.0 %fused.1 = bf16[256,1024]{1,0:T(8,128)(2,1)S(1)} custom-call(bf16[256,512]{1,0:T(8,128)(2,1)} %q_hbm.1, bf16[256,512]{1,0:T(8,128)(2,1)} %k_hbm.1, bf16[256,512]{1,0:T(8,128)(2,1)} %v_hbm.1), custom_call_target="tpu_custom_call" | custom-call | tf_op jit(solution)/shard_map/fused/pallas_call | solution.py:351
  33.0 0.0 copy-done
  33.0 1.5 %convolution_convert_fusion = bf16[256,1024]{1,0:T(8,128)(2,1)} fusion(bf16[256,1024]{1,0:T(8,128)(2,1)S(1)} %fused.1, bf16[1024,1024]{1,0:T(8,128)(2,1)S(1)} %copy-done), kind=kOutput, calls=%fused_computation | convolution fusion | flops 537133056 | bytes 3145728 | tf_op jit(solution)/shard_map/dot_general | solution.py:392
Async XLA Ops:
  0.0 33.0 %copy-start = (bf16[1024,1024]{1,0:T(8,128)(2,1)S(1)}, bf16[1024,1024]{1,0:T(8,128)(2,1)}, u32[]{:S(2)}) copy-start(bf16[1024,1024]{1,0:T(8,128)(2,1)} %param.7) | copy-start | bytes 6291460

commit v4 on v3

--- a/solution.py
+++ b/solution.py
@@ -19,6 +19,7 @@
 NEG = -1e30
 COEF = math.log2(math.e) / math.sqrt(HEAD_DIM)
 PEERS = (1, 3, 2)
+SENDS = (2, 1, 3)
 
 
 def attend(q, k, v, bias):
@@ -28,7 +29,7 @@
     p = jnp.exp2(t - m)
     l = jnp.sum(p, axis=1, keepdims=True)
     acc = jnp.dot(p.astype(BF), v, preferred_element_type=F32)
-    return m, l, acc
+    return jnp.broadcast_to(m, acc.shape), jnp.broadcast_to(l, acc.shape), acc
 
 
 def kernel(
@@ -145,8 +146,8 @@
             def _():
                 taken(kvres.at[h, pl.ds(0, ROW)], yr.at[h, way])
 
-    def halo_send():
-        for way, side in enumerate(halo_out):
+    def halo_send(sides):
+        for way, side in enumerate(sides):
             @pl.when(side)
             def _():
                 for a in (kn, vn):
@@ -165,8 +166,8 @@
     y_out, y_in = (to_up, to_down), (to_down, to_up)
     halo_out, halo_in = (to_right, to_left), (to_left, to_right)
 
-    for h in range(heads):
-        for k in PEERS:
+    for h in range(heads - 1):
+        for k in SENDS:
             x_kv(h, k).start()
     y_send([(h, 0) for h in range(heads)])
     with scope("load_q"):
@@ -176,8 +177,12 @@
         for c in range(ROW):
             xq[c, h] = cut(qp, c, h)
     for h in range(heads):
-        for k in PEERS:
+        for k in SENDS:
             x_q(h, k).start()
+        if h == 0:
+            for k in SENDS:
+                x_kv(heads - 1, k).start()
+    halo_send((to_right & (x < ROW - 1), to_left & (x > 0)))
     for h in range(heads):
         kvres[h, ROW + x] = xkv[x, h]
         qres[h, x] = xq[x, h]
@@ -244,11 +249,13 @@
             remote(sstat.at[h, s], rstat.at[h, x], rs.at[1], rr.at[h, 1], (base + s, tp)),
         ]
 
-    def residue(h):
+    def residue_wait(h):
         with scope(f"wait_q_{h}"):
             taken(qres.at[h, pl.ds(0, ROW - 1)], qr.at[h])
         with scope(f"wait_y_{h}"):
             y_wait(h)
+
+    def residue_work(h):
         far, mid = [], []
         for e in range(2):
             two = slice(2 * e, 2 * e + 2)
@@ -260,6 +267,7 @@
             k = kvres[h, 2 * e + 3 : 2 * e + 7, 0].reshape(4 * SIDE, HEAD_DIM)
             v = kvres[h, 2 * e + 3 : 2 * e + 7, 1].reshape(4 * SIDE, HEAD_DIM)
             mid.append(attend(q, k, v, mid_bias[e]))
+        lses = []
         for s in range(ROW):
             part = slice(s % 2 * SIDE, (s % 2 + 1) * SIDE)
             m1, l1, acc1 = (mid[s // 2][i][part] for i in range(3))
@@ -270,16 +278,25 @@
             m = jnp.maximum(m1, m2)
             a1, a2 = jnp.exp2(m1 - m), jnp.exp2(m2 - m)
             l = a1 * l1 + a2 * l2
-            inv = 1.0 / l
-            sret[h, s] = ((a1 * inv) * acc1 + (a2 * inv) * acc2).astype(BF)
-            lse = jnp.broadcast_to(m + jnp.log2(l), (SIDE, HEAD_DIM))
-            flat = jnp.transpose(jnp.concatenate([lse, lse], axis=0))
-            sstat[h, s] = flat[:1]
-        for k in PEERS:
-            for copy in give_back(h, k):
-                copy.start()
-        ret[h, x] = sret[h, x]
-        rstat[h, x] = sstat[h, x]
+            sret[h, s] = ((a1 * acc1 + a2 * acc2) / l).astype(BF)
+            lses.append(m + jnp.log2(l))
+        for e in range(2):
+            flat = jnp.transpose(jnp.concatenate(lses[2 * e : 2 * e + 2], axis=0))
+            sstat[h, 2 * e] = flat[:1]
+            sstat[h, 2 * e + 1] = flat[:1]
+
+    def residue(*which):
+        for h in which:
+            residue_wait(h)
+        for h in which:
+            residue_work(h)
+        for h in which:
+            for k in SENDS:
+                for copy in give_back(h, k):
+                    copy.start()
+        for h in which:
+            ret[h, x] = sret[h, x]
+            rstat[h, x] = sstat[h, x]
 
     def columns(h, side):
         return pl.ds(pl.multiple_of((side * heads + h) * HEAD_DIM, HEAD_DIM), HEAD_DIM)
@@ -296,31 +313,30 @@
         out = jnp.dot(unperm, got, preferred_element_type=F32)
         lane = iota((rows, HEAD_DIM), 1)
         small = iota((1, HEAD_DIM), 1)
+        odd = jnp.broadcast_to(x & 1, (1, HEAD_DIM)) == 1
         where = lead[...]
         col = jnp.zeros((rows, HEAD_DIM), F32)
         for pair in range(2):
-            row = jnp.where(
-                small < piece, rstat[h, 2 * pair], rstat[h, 2 * pair + 1]
-            )
+            one, two = rstat[h, 2 * pair], rstat[h, 2 * pair + 1]
+            one = jnp.where(odd, pltpu.roll(one, SIDE, 1), one)
+            two = jnp.where(odd, two, pltpu.roll(two, SIDE, 1))
+            row = jnp.where(small < piece, one, two)
             col = jnp.where(where == lane + pair * HEAD_DIM, row, col)
-        lse = jnp.sum(col, axis=1, keepdims=True)
+        lse = jnp.broadcast_to(jnp.sum(col, axis=1, keepdims=True), col.shape)
         m0 = nm[h]
         m = jnp.maximum(m0, lse)
         a0, a1 = jnp.exp2(m0 - m), jnp.exp2(lse - m)
-        inv = 1.0 / (a0 * nl[h] + a1)
-        att = (a0 * inv) * nacc[h] + (a1 * inv) * out
+        att = (a0 * nacc[h] + a1 * out) / (a0 * nl[h] + a1)
         out_ref[:, columns(h, tp)] = att.astype(BF)
         tp_copy(h).start()
 
     relay(0)
     relay(1)
     relay(2)
-    residue(0)
     relay(3)
-    halo_send()
-    residue(1)
-    residue(2)
-    residue(3)
+    halo_send((to_right & (x == ROW - 1), to_left & (x == 0)))
+    for h in range(heads):
+        residue(h)
     with scope("wait_halo"):
         halo_wait(nr, halo_in)
     for h in range(heads):
@@ -366,8 +382,8 @@
             vmem((heads, ROW, SIDE, HEAD_DIM), BF),
             vmem((heads, ROW, 1, HEAD_DIM), F32),
             vmem((heads, rows, HEAD_DIM), F32),
-            vmem((heads, rows, 1), F32),
-            vmem((heads, rows, 1), F32),
+            vmem((heads, rows, HEAD_DIM), F32),
+            vmem((heads, rows, HEAD_DIM), F32),
             vmem((2, 2 * SIDE, 4 * SIDE), F32),
             vmem((2, 2 * SIDE, 4 * SIDE), F32),
             vmem((2 * SIDE, 6 * SIDE), F32),

time: 34.7 us -> 33.3 us (0.960)
  Pallas kernels: 33 us -> 31.7 us
    pallas_call x1, Pallas kernels: 33 us -> 31.7 us  [per_device(): pl.pallas_call(functools.partial(kernel, n, heads), out_shape=jax.ShapeDt...]
where the time goes in v4:
time: 33.3 us; the launch traced here: 33.2 us
  Pallas kernels  31.7 us (95%)
  matrix products  1.51 us (5%)
    pallas_call x1, Pallas kernels, per_device(): pl.pallas_call(functools.partial(kernel, n, heads), out_shape=jax.ShapeDt...  31.7 us
    dot_general x1, matrix products, per_device(): return jnp.dot(attended, w_out, preferred_element_type=F32).astype(BF)  1.51 us

profile of v4, /device:TPU:1, one launch (start us, length us, event | category | flops | bytes accessed | tf_op | source)
XLA Modules:
  0.0 33.2 jit_solution(7721677133661102490)
XLA Ops:
  0.0 0.0 copy-start
  0.0 31.7 %fused.1 = bf16[256,1024]{1,0:T(8,128)(2,1)S(1)} custom-call(bf16[256,512]{1,0:T(8,128)(2,1)} %q_hbm.1, bf16[256,512]{1,0:T(8,128)(2,1)} %k_hbm.1, bf16[256,512]{1,0:T(8,128)(2,1)} %v_hbm.1), custom_call_target="tpu_custom_call" | custom-call | tf_op jit(solution)/shard_map/fused/pallas_call | solution.py:367
  31.7 0.0 copy-done
  31.7 1.5 %convolution_convert_fusion = bf16[256,1024]{1,0:T(8,128)(2,1)} fusion(bf16[256,1024]{1,0:T(8,128)(2,1)S(1)} %fused.1, bf16[1024,1024]{1,0:T(8,128)(2,1)S(1)} %copy-done), kind=kOutput, calls=%fused_computation | convolution fusion | flops 537133056 | bytes 3145728 | tf_op jit(solution)/shard_map/dot_general | solution.py:408
Async XLA Ops:
  0.0 31.7 %copy-start = (bf16[1024,1024]{1,0:T(8,128)(2,1)S(1)}, bf16[1024,1024]{1,0:T(8,128)(2,1)}, u32[]{:S(2)}) copy-start(bf16[1024,1024]{1,0:T(8,128)(2,1)} %param.7) | copy-start | bytes 6291460

commit v5 on v4

--- a/solution.py
+++ b/solution.py
@@ -19,7 +19,7 @@
 NEG = -1e30
 COEF = math.log2(math.e) / math.sqrt(HEAD_DIM)
 PEERS = (1, 3, 2)
-SENDS = (2, 1, 3)
+SENDS = (1, 3, 2)
 
 
 def attend(q, k, v, bias):
@@ -218,11 +218,9 @@
     band = (wk - wq <= SIDE) & (wq - wk <= SIDE)
     mid_bias[0] = jnp.where(band & (ik >= low), 0.0, NEG)
     mid_bias[1] = jnp.where(band & (ik < high), 0.0, NEG)
-    iq, ik = iota((2 * SIDE, 6 * SIDE), 0), iota((2 * SIDE, 6 * SIDE), 1)
-    vq = (iq >> 5) * BLK + (iq & 15)
-    vk = (ik >> 5) * BLK + (ik & 15)
-    band = (vk >= vq) & (vk <= vq + 2 * SIDE) & ((iq & 16) == (ik & 16))
-    band = band & (vk >= first * SIDE) & (vk < (3 - last) * SIDE)
+    iq = iq & (SIDE - 1)
+    band = (ik >= iq) & (ik <= iq + 2 * SIDE)
+    band = band & (ik >= first * SIDE) & (ik < (3 - last) * SIDE)
     far_bias[...] = jnp.where(band, 0.0, NEG)
     lead[...] = place[:, :HEAD_DIM]
 
@@ -257,12 +255,16 @@
 
     def residue_work(h):
         far, mid = [], []
+        for d in range(SUB):
+            q = qres[h, :, d].reshape(SIDE, HEAD_DIM)
+            k = kvres[h, :, 0, d].reshape(3 * SIDE, HEAD_DIM)
+            v = kvres[h, :, 1, d].reshape(3 * SIDE, HEAD_DIM)
+            q = jnp.concatenate([q, q], axis=0)
+            k = jnp.concatenate([k, k[:SIDE]], axis=0)
+            v = jnp.concatenate([v, v[:SIDE]], axis=0)
+            far.append([a[:SIDE] for a in attend(q, k, v, far_bias[...])])
         for e in range(2):
             two = slice(2 * e, 2 * e + 2)
-            q = qres[h, :, two].reshape(2 * SIDE, HEAD_DIM)
-            k = kvres[h, :, 0, two].reshape(6 * SIDE, HEAD_DIM)
-            v = kvres[h, :, 1, two].reshape(6 * SIDE, HEAD_DIM)
-            far.append(attend(q, k, v, far_bias[...]))
             q = qres[h, two].reshape(2 * SIDE, HEAD_DIM)
             k = kvres[h, 2 * e + 3 : 2 * e + 7, 0].reshape(4 * SIDE, HEAD_DIM)
             v = kvres[h, 2 * e + 3 : 2 * e + 7, 1].reshape(4 * SIDE, HEAD_DIM)
@@ -271,7 +273,7 @@
         for s in range(ROW):
             part = slice(s % 2 * SIDE, (s % 2 + 1) * SIDE)
             m1, l1, acc1 = (mid[s // 2][i][part] for i in range(3))
-            part = slice(s * 2 * BLK, (s + 1) * 2 * BLK)
+            part = slice(s * BLK, (s + 1) * BLK)
             m2, l2, acc2 = (
                 jnp.concatenate([f[i][part] for f in far], axis=0) for i in range(3)
             )
@@ -386,7 +388,7 @@
             vmem((heads, rows, HEAD_DIM), F32),
             vmem((2, 2 * SIDE, 4 * SIDE), F32),
             vmem((2, 2 * SIDE, 4 * SIDE), F32),
-            vmem((2 * SIDE, 6 * SIDE), F32),
+            vmem((2 * SIDE, 4 * SIDE), F32),
             vmem((rows, HEAD_DIM), jnp.int32),
             dma((3,)),
             dma((2,)),

time: 33.3 us -> 32.1 us (0.964)
  Pallas kernels: 31.7 us -> 30.2 us
    pallas_call x1, Pallas kernels: 31.7 us -> 30.2 us  [per_device(): pl.pallas_call(functools.partial(kernel, n, heads), out_shape=jax.ShapeDt...]
where the time goes in v5:
time: 32.1 us; the launch traced here: 31.7 us
  Pallas kernels  30.2 us (94%)
  matrix products  1.51 us (5%)
    pallas_call x1, Pallas kernels, per_device(): pl.pallas_call(functools.partial(kernel, n, heads), out_shape=jax.ShapeDt...  30.2 us
    dot_general x1, matrix products, per_device(): return jnp.dot(attended, w_out, preferred_element_type=F32).astype(BF)  1.51 us

profile of v5, /device:TPU:1, one launch (start us, length us, event | category | flops | bytes accessed | tf_op | source)
XLA Modules:
  0.0 31.7 jit_solution(9328587739055032543)
XLA Ops:
  0.0 0.0 copy-start
  0.0 30.2 %fused.1 = bf16[256,1024]{1,0:T(8,128)(2,1)S(1)} custom-call(bf16[256,512]{1,0:T(8,128)(2,1)} %q_hbm.1, bf16[256,512]{1,0:T(8,128)(2,1)} %k_hbm.1, bf16[256,512]{1,0:T(8,128)(2,1)} %v_hbm.1), custom_call_target="tpu_custom_call" | custom-call | tf_op jit(solution)/shard_map/fused/pallas_call | solution.py:369
  30.2 0.0 copy-done
  30.2 1.5 %convolution_convert_fusion = bf16[256,1024]{1,0:T(8,128)(2,1)} fusion(bf16[256,1024]{1,0:T(8,128)(2,1)S(1)} %fused.1, bf16[1024,1024]{1,0:T(8,128)(2,1)S(1)} %copy-done), kind=kOutput, calls=%fused_computation | convolution fusion | flops 537133056 | bytes 3145728 | tf_op jit(solution)/shard_map/dot_general | solution.py:410
Async XLA Ops:
  0.0 30.2 %copy-start = (bf16[1024,1024]{1,0:T(8,128)(2,1)S(1)}, bf16[1024,1024]{1,0:T(8,128)(2,1)}, u32[]{:S(2)}) copy-start(bf16[1024,1024]{1,0:T(8,128)(2,1)} %param.7) | copy-start | bytes 6291460

commit v6 on v5

--- a/solution.py
+++ b/solution.py
@@ -166,23 +166,29 @@
     y_out, y_in = (to_up, to_down), (to_down, to_up)
     halo_out, halo_in = (to_right, to_left), (to_left, to_right)
 
-    for h in range(heads - 1):
-        for k in SENDS:
-            x_kv(h, k).start()
-    y_send([(h, 0) for h in range(heads)])
+    def first_sends():
+        for h in range(heads - 1):
+            for k in SENDS:
+                x_kv(h, k).start()
+        y_send([(h, 0) for h in range(heads)])
+
+    def second_sends():
+        for h in range(heads):
+            for k in SENDS:
+                x_q(h, k).start()
+            if h == 0:
+                for k in SENDS:
+                    x_kv(heads - 1, k).start()
+        halo_send((to_right & (x < ROW - 1), to_left & (x > 0)))
+
+    pl.when(tp == 0)(first_sends)
     with scope("load_q"):
         loads[2].wait()
     qp = jnp.dot(perm, qn[...], preferred_element_type=F32).astype(BF)
     for h in range(heads):
         for c in range(ROW):
             xq[c, h] = cut(qp, c, h)
-    for h in range(heads):
-        for k in SENDS:
-            x_q(h, k).start()
-        if h == 0:
-            for k in SENDS:
-                x_kv(heads - 1, k).start()
-    halo_send((to_right & (x < ROW - 1), to_left & (x > 0)))
+    pl.when(tp == 0)(second_sends)
     for h in range(heads):
         kvres[h, ROW + x] = xkv[x, h]
         qres[h, x] = xq[x, h]
@@ -224,21 +230,25 @@
     far_bias[...] = jnp.where(band, 0.0, NEG)
     lead[...] = place[:, :HEAD_DIM]
 
+    @pl.when(tp == 1)
+    def _():
+        first_sends()
+        second_sends()
+
     def relay(h):
         for k in PEERS:
             with scope(f"relay_{h}_{k}"):
                 x_kv(h, k).wait_recv()
             y_send([(h, k)])
 
-    def near(h):
+    def near(h, b):
         cols = slice(h * HEAD_DIM, (h + 1) * HEAD_DIM)
-        for b in range(2):
-            span = slice(b * 2 * SIDE, (b + 1) * 2 * SIDE)
-            keys = slice(b * 2 * SIDE, b * 2 * SIDE + 4 * SIDE)
-            m, l, acc = attend(qn[span, cols], kn[keys, cols], vn[keys, cols], near_bias[b])
-            nm[h, span] = m
-            nl[h, span] = l
-            nacc[h, span] = acc
+        span = slice(b * 2 * SIDE, (b + 1) * 2 * SIDE)
+        keys = slice(b * 2 * SIDE, b * 2 * SIDE + 4 * SIDE)
+        m, l, acc = attend(qn[span, cols], kn[keys, cols], vn[keys, cols], near_bias[b])
+        nm[h, span] = m
+        nl[h, span] = l
+        nacc[h, span] = acc
 
     def give_back(h, k):
         s = xpeer(k)
@@ -339,10 +349,11 @@
     halo_send((to_right & (x == ROW - 1), to_left & (x == 0)))
     for h in range(heads):
         residue(h)
-    with scope("wait_halo"):
-        halo_wait(nr, halo_in)
-    for h in range(heads):
-        near(h)
+    for b in (1, 0):
+        with scope(f"wait_halo_{b}"):
+            halo_wait(nr, tuple(side if way == b else sp < 0 for way, side in enumerate(halo_in)))
+        for h in range(heads):
+            near(h, b)
     for h in range(heads):
         combine(h)
 

time: 32.1 us -> 32.1 us (level)
  no operation moved by 1% of the time
where the time goes in v6:
time: 32.1 us; the launch traced here: 31.7 us
  Pallas kernels  30.2 us (94%)
  matrix products  1.51 us (5%)
    pallas_call x1, Pallas kernels, per_device(): pl.pallas_call(functools.partial(kernel, n, heads), out_shape=jax.ShapeDt...  30.2 us
    dot_general x1, matrix products, per_device(): return jnp.dot(attended, w_out, preferred_element_type=F32).astype(BF)  1.51 us

profile of v6, /device:TPU:1, one launch (start us, length us, event | category | flops | bytes accessed | tf_op | source)
XLA Modules:
  0.0 31.7 jit_solution(12835407284228101204)
XLA Ops:
  0.0 0.0 copy-start
  0.0 30.2 %fused.1 = bf16[256,1024]{1,0:T(8,128)(2,1)S(1)} custom-call(bf16[256,512]{1,0:T(8,128)(2,1)} %q_hbm.1, bf16[256,512]{1,0:T(8,128)(2,1)} %k_hbm.1, bf16[256,512]{1,0:T(8,128)(2,1)} %v_hbm.1), custom_call_target="tpu_custom_call" | custom-call | tf_op jit(solution)/shard_map/fused/pallas_call | solution.py:380
  30.2 0.0 copy-done
  30.2 1.5 %convolution_convert_fusion = bf16[256,1024]{1,0:T(8,128)(2,1)} fusion(bf16[256,1024]{1,0:T(8,128)(2,1)S(1)} %fused.1, bf16[1024,1024]{1,0:T(8,128)(2,1)S(1)} %copy-done), kind=kOutput, calls=%fused_computation | convolution fusion | flops 537133056 | bytes 3145728 | tf_op jit(solution)/shard_map/dot_general | solution.py:421
Async XLA Ops:
  0.0 30.2 %copy-start = (bf16[1024,1024]{1,0:T(8,128)(2,1)S(1)}, bf16[1024,1024]{1,0:T(8,128)(2,1)}, u32[]{:S(2)}) copy-start(bf16[1024,1024]{1,0:T(8,128)(2,1)} %param.7) | copy-start | bytes 6291460
